TPU v7x, 32 devices: a whole 2x2x4 slice. The times are simulated.
32 devices in a mesh: ep: 16 (over z, y, core), tp: 2 (over x).
Axes of the slice: x: 2, y: 2, z: 4, core: 2. Of those that a mesh axis runs over, the one named last changes fastest.
Arguments:
- tokens: bfloat16 [256, 2048], P('ep'), may hold values from -6 to 6
- lengths: int32 [256], P('ep'), may hold values from 256 to 1023
- cache: bfloat16 [256, 1024, 512], P('ep', None, 'tp'), may hold values from -6 to 6
- attn_gain: float32 [2048], replicated, may hold values from 0.1 to 1.9
- query_weight: bfloat16 [2048, 1024], P(None, 'tp'), may hold values from -0.125 to 0.125
- key_weight: bfloat16 [2048, 256], P(None, 'tp'), may hold values from -0.125 to 0.125
- value_weight: bfloat16 [2048, 256], P(None, 'tp'), may hold values from -0.125 to 0.125
- stick_bias: float32 [16], P('tp'), may hold values from -7 to -1
- out_weight: bfloat16 [1024, 2048], P('tp'), may hold values from -0.1875 to 0.1875
- ffn_gain: float32 [2048], replicated, may hold values from 0.1 to 1.9
- routes: int32 [256, 6], P('ep'), may hold values from 0 to 15, all different within a row; in each aligned block of 16 rows (0 to 15, 16 to 31, ...) at most 12 rows name the same one
- route_weights: float32 [256, 6], P('ep'), may hold values from 0.1 to 0.6
- expert_gate: bfloat16 [16, 2048, 1024], P('ep', None, 'tp'), may hold values from -0.125 to 0.125
- expert_up: bfloat16 [16, 2048, 1024], P('ep', None, 'tp'), may hold values from -0.125 to 0.125
- expert_down: bfloat16 [16, 1024, 2048], P('ep', 'tp'), may hold values from -0.1875 to 0.1875
- shared_gate: bfloat16 [2048, 512], P('ep', 'tp'), may hold values from -0.125 to 0.125
- shared_up: bfloat16 [2048, 512], P('ep', 'tp'), may hold values from -0.125 to 0.125
- shared_down: bfloat16 [512, 2048], P('tp'), may hold values from -0.25 to 0.25
- gate_vector: bfloat16 [2048], replicated, may hold values from -0.125 to 0.125
Outputs:
- layer_out: bfloat16 [256, 2048], P('ep', 'tp')
- new_kv: bfloat16 [256, 512], P('ep', 'tp')
Inputs may be any that keep to these rules, and one draw needn't show every extreme that they name: Each sequence's new token comes after its lengths cached positions. `routes`: each row names 6 different experts; among the 16 rows of one index of ep no expert is named by more than 12 rows.
All inputs are finite; a program needn't handle non-finite values.
Results may differ from a plain program's by a relative error of at most 0.012.
Values may be sent and summed in bfloat16 or wider, within the bound.
A program may use at most 64 MiB of HBM per device.

v0:
```python
import jax
import jax.numpy as jnp
from jax import lax
from jax.sharding import PartitionSpec as P

HEAD_DIM = 64


epsilon = 1e-06


def rms_scale(rows_in, gain_row):
    values_f = rows_in.astype(jnp.float32)
    return (
        values_f
        * lax.rsqrt(jnp.mean(values_f * values_f, axis=-1, keepdims=True) + epsilon)
        * gain_row
    )


def later_sum(values):
    lead = values.shape[:-1]
    length = values.shape[-1]
    width = 128
    count = length // width
    blocked = values.reshape(lead + (count, width))
    inner_rows = lax.broadcasted_iota(jnp.int32, (width, width), 0)
    inner_cols = lax.broadcasted_iota(jnp.int32, (width, width), 1)
    inner_table = (inner_rows > inner_cols).astype(jnp.float32)
    within = jnp.einsum("...bj,js->...bs", blocked, inner_table, precision=lax.Precision.HIGHEST)
    totals = jnp.sum(blocked, axis=-1)
    outer_rows = lax.broadcasted_iota(jnp.int32, (count, count), 0)
    outer_cols = lax.broadcasted_iota(jnp.int32, (count, count), 1)
    outer_table = (outer_rows > outer_cols).astype(jnp.float32)
    beyond = jnp.einsum("...j,ji->...i", totals, outer_table, precision=lax.Precision.HIGHEST)
    return (within + beyond[..., None]).reshape(lead + (length,))


def shards(
    tokens,
    lengths,
    cache,
    attn_gain,
    query_weight,
    key_weight,
    value_weight,
    stick_bias,
    out_weight,
    ffn_gain,
    routes,
    route_weights,
    expert_gate,
    expert_up,
    expert_down,
    shared_gate,
    shared_up,
    shared_down,
    gate_vector,
):
    ranks_tp = lax.axis_size("tp")
    ranks_ep = lax.axis_size("ep")
    row_count = tokens.shape[0]
    model_width = tokens.shape[1]
    quarter = model_width // ranks_tp
    part_index = lax.axis_index("tp")
    normed = rms_scale(tokens, attn_gain).astype(jnp.bfloat16)
    queries = jnp.dot(normed, query_weight, preferred_element_type=jnp.float32).astype(jnp.bfloat16)
    key_rows = jnp.dot(normed, key_weight, preferred_element_type=jnp.float32).astype(jnp.bfloat16)
    value_rows = jnp.dot(normed, value_weight, preferred_element_type=jnp.float32).astype(
        jnp.bfloat16
    )
    local_heads = key_weight.shape[1] // HEAD_DIM
    new_kv = jnp.stack(
        [
            key_rows.reshape(row_count, local_heads, HEAD_DIM),
            value_rows.reshape(row_count, local_heads, HEAD_DIM),
        ],
        axis=2,
    )
    new_kv = new_kv.reshape(row_count, local_heads * 2 * HEAD_DIM)
    group_size = queries.shape[1] // HEAD_DIM // local_heads
    grouped = queries.reshape(row_count, local_heads, group_size, HEAD_DIM)
    cache_len = cache.shape[1]
    cache_view = cache.reshape(row_count, cache_len, local_heads, 2, HEAD_DIM)
    scores = jnp.einsum(
        "nkgd,nckd->nkgc", grouped, cache_view[:, :, :, 0, :], preferred_element_type=jnp.float32
    ) * HEAD_DIM ** (-0.5)
    scores = scores + stick_bias.reshape(1, local_heads, group_size, 1)
    positions = lax.broadcasted_iota(jnp.int32, (1, 1, 1, cache_len), 3)
    usable = positions < lengths.reshape(row_count, 1, 1, 1)
    log_keep = jnp.where(usable, jax.nn.log_sigmoid(-scores), 0.0)
    behind = later_sum(log_keep)
    stick_weights = jnp.where(usable, jnp.exp(jax.nn.log_sigmoid(scores) + behind), 0.0).astype(
        jnp.bfloat16
    )
    heads_out = jnp.einsum(
        "nkgc,nckd->nkgd",
        stick_weights,
        cache_view[:, :, :, 1, :],
        preferred_element_type=jnp.float32,
    ).astype(jnp.bfloat16)
    attn_term = jnp.dot(
        heads_out.reshape(row_count, -1), out_weight, preferred_element_type=jnp.float32
    )
    attn_share = lax.psum_scatter(
        attn_term.astype(jnp.bfloat16), "tp", scatter_dimension=1, tiled=True
    ).astype(jnp.float32)
    own_tokens = lax.dynamic_slice_in_dim(tokens, part_index * quarter, quarter, 1)
    residual = own_tokens.astype(jnp.float32) + attn_share
    stat_total = lax.psum(jnp.sum(residual * residual, axis=1), "tp")
    own_gain = lax.dynamic_slice_in_dim(ffn_gain, part_index * quarter, quarter, 0)
    inverse = lax.rsqrt(stat_total / model_width + epsilon)
    normed_part = (residual * inverse[:, None] * own_gain).astype(jnp.bfloat16)
    normed_mix = lax.all_gather(normed_part, "tp", axis=1, tiled=True)
    route_count = routes.shape[1]
    local_experts = expert_gate.shape[0]
    experts_all = ranks_ep * local_experts
    capacity = min(row_count, max(2, 2 * row_count * route_count // experts_all))
    slot_total = experts_all * capacity
    flat_routes = routes.reshape(-1)
    flat_count = flat_routes.shape[0]
    expert_hits = (
        flat_routes[:, None] == lax.broadcasted_iota(jnp.int32, (1, experts_all), 1)
    ).astype(jnp.float32)
    lower_table = (
        lax.broadcasted_iota(jnp.int32, (flat_count, flat_count), 0)
        > lax.broadcasted_iota(jnp.int32, (flat_count, flat_count), 1)
    ).astype(jnp.float32)
    earlier = jnp.dot(lower_table, expert_hits, precision=lax.Precision.HIGHEST)
    slot_rank = jnp.sum(earlier * expert_hits, axis=1).astype(jnp.int32)
    slot_index = flat_routes * capacity + slot_rank
    owned_slots = slot_index[:, None] == lax.broadcasted_iota(jnp.int32, (1, slot_total), 1)
    owned_slots = owned_slots.reshape(row_count, route_count, slot_total)
    take_matrix = jnp.any(owned_slots, axis=1).astype(jnp.bfloat16)
    mix_weights = jnp.sum(owned_slots.astype(jnp.float32) * route_weights[:, :, None], axis=1)
    pick_dims = (((0,), (0,)), ((), ()))
    sent_rows = lax.dot_general(
        take_matrix, normed_mix, pick_dims, preferred_element_type=jnp.float32
    ).astype(jnp.bfloat16)
    arrived = lax.all_to_all(sent_rows, "ep", split_axis=0, concat_axis=0, tiled=True)
    expert_grid = arrived.reshape(ranks_ep, local_experts, capacity, model_width)
    gate_val = jnp.einsum(
        "sjcd,jdf->sjcf", expert_grid, expert_gate, preferred_element_type=jnp.float32
    )
    up_val = jnp.einsum(
        "sjcd,jdf->sjcf", expert_grid, expert_up, preferred_element_type=jnp.float32
    )
    expert_hidden = (jax.nn.silu(gate_val) * up_val).astype(jnp.bfloat16)
    expert_term = jnp.einsum(
        "sjcf,jfd->sjcd", expert_hidden, expert_down, preferred_element_type=jnp.float32
    )
    expert_term = expert_term.reshape(-1, model_width)
    shared_width = shared_gate.shape[1]
    column_rows = lax.all_to_all(normed_mix, "ep", split_axis=1, concat_axis=0, tiled=True)
    joined_weights = jnp.concatenate([shared_gate, shared_up], axis=1)
    dense_total = lax.psum_scatter(
        jnp.dot(column_rows, joined_weights, preferred_element_type=jnp.float32),
        "ep",
        scatter_dimension=0,
        tiled=True,
    )
    gate_sum = dense_total[:, :shared_width]
    up_sum = dense_total[:, shared_width:]
    shared_hidden = (jax.nn.silu(gate_sum) * up_sum).astype(jnp.bfloat16)
    shared_term = jnp.dot(shared_hidden, shared_down, preferred_element_type=jnp.float32)
    expert_share, shared_share = (
        lax.psum_scatter(
            expert_term.astype(jnp.bfloat16), "tp", scatter_dimension=1, tiled=True
        ).astype(jnp.float32),
        lax.psum_scatter(
            shared_term.astype(jnp.bfloat16), "tp", scatter_dimension=1, tiled=True
        ).astype(jnp.float32),
    )
    expert_out = expert_share.astype(jnp.bfloat16).reshape(
        ranks_ep, local_experts * capacity, quarter
    )
    returned = lax.all_to_all(expert_out, "ep", split_axis=0, concat_axis=0, tiled=True).reshape(
        slot_total, quarter
    )
    routed = jnp.dot(mix_weights, returned.astype(jnp.float32), precision=lax.Precision.HIGHEST)
    mix_gate = jax.nn.sigmoid(jnp.dot(normed_mix, gate_vector, preferred_element_type=jnp.float32))
    layer_out = (residual + routed + mix_gate[:, None] * shared_share).astype(jnp.bfloat16)
    return (layer_out, new_kv)


def solution(mesh):
    placed = (
        P("ep", None),
        P("ep"),
        P("ep", None, "tp"),
        P(),
        P(None, "tp"),
        P(None, "tp"),
        P(None, "tp"),
        P("tp"),
        P("tp", None),
        P(),
        P("ep", None),
        P("ep", None),
        P("ep", None, "tp"),
        P("ep", None, "tp"),
        P("ep", "tp", None),
        P("ep", "tp"),
        P("ep", "tp"),
        P("tp", None),
        P(),
    )
    return jax.shard_map(
        shards,
        mesh=mesh,
        in_specs=placed,
        out_specs=(P("ep", "tp"), P("ep", "tp")),
        check_vma=False,
    )
```

profile of v0, /device:TPU:0, one launch (start us, length us, event | category | flops | bytes accessed | tf_op | source)
XLA Modules:
  0.0 192.9 jit_solution(2589733550012871538)
XLA Ops:
  7.2 1.1 fusion.44
  8.3 2.1 %convolution_convert_fusion.4 = bf16[16,512]{1,0:T(8,128)(2,1)S(1)} fusion(bf16[2048,512]{1,0:T(8,128)(2,1)} %param.23, bf16[16,2048]{1,0:T(8,128)(2,1)} %param.19, f32[2048]{0:T(1024)} %param.22, f32[16]{0:T(128)S(1)} %add_rsqrt_fusion.1), kind=kOutput, calls=%fused_computation.28 | convolution fusion | flops 33693696 | bytes 2187328 | tf_op jit(solution)/shard_map/dot_general | solution.py:67
  10.5 12.3 %copy.63 = bf16[16,1024,256]{1,2,0:T(8,128)(2,1)} copy(bf16[16,1024,256]{2,1,0:T(8,128)(2,1)} %param.21) | data formatting | bytes 16777216 | tf_op args[2]
  23.0 4.1 %fusion.39 = (f32[16,2,4,1024]{3,2,1,0:T(4,128)S(1)}, f32[16,2,4,1024]{3,2,1,0:T(4,128)}) fusion(pred[16,1024]{1,0:T(8,128)(4,1)S(1)} %iota_compare_fusion.2, f32[2,4]{1,0:T(2,128)S(1)} %add.83, bf16[16,2,4,64]{3,2,1,0:T(4,128)(2,1)S(1)} %reshape.116, bf16[16,1024,2,2,64]{1,4,3,2,0:T(8,128)(2,1)} %bitcast.116), kind=kOutput, calls=%fused_computation.44 | convolution fusion | flops 18087936 | bytes 5275680 | tf_op jit(solution)/shard_map/nkgd,nckd->nkgc/dot_general | solution.py:85
  27.5 0.3 fusion.52
  28.0 0.4 convolution_add_fusion
  28.6 3.6 %fusion.27 = bf16[16,2,4,64]{3,2,1,0:T(4,128)(2,1)S(1)} fusion(bf16[16,1024,2,2,64]{1,4,3,2,0:T(8,128)(2,1)} %bitcast.117, f32[16,2,4,1024]{3,2,1,0:T(4,128)S(1)} %reshape.119, f32[16,2,4,1024]{3,2,1,0:T(4,128)} %get-tuple-element.3, pred[16,1024]{1,0:T(8,128)(4,1)S(1)} %iota_compare_fusion.2), kind=kOutput, calls=%fused_computation.27 | convolution fusion | flops 18227200 | bytes 5275648 | tf_op jit(solution)/shard_map/nkgc,nckd->nkgd/dot_general | solution.py:96
  32.3 2.6 %convolution_convert_fusion.3 = bf16[16,2048]{1,0:T(8,128)(2,1)} fusion(bf16[16,512]{1,0:T(8,128)(2,1)S(1)} %reshape.120, bf16[512,2048]{1,0:T(8,128)(2,1)} %param.27), kind=kOutput, calls=%fused_computation.8 | convolution fusion | flops 33587200 | bytes 2179072 | tf_op jit(solution)/shard_map/dot_general | solution.py:102
  35.6 12.2 %reduce-scatter.5.cloned.1.call-done = bf16[16,1024]{1,0:T(8,128)(2,1)} async-done(((bf16[16,2048]{1,0:T(8,128)(2,1)}), bf16[16,1024]{1,0:T(8,128)(2,1)}) %reduce-scatter.5.cloned.1.call-update) | async-done | bytes 32784 | tf_op jit(solution)/shard_map/reduce_scatter | solution.py:105
  47.8 0.9 multiply_reduce_fusion
  48.7 4.9 %psum.7 = f32[16]{0:T(128)S(1)} all-reduce(f32[16]{0:T(128)S(1)} %multiply_reduce_fusion), channel_id=1, replica_groups=mesh['ep'=16,'tp'=2] {'tp'}, use_global_device_ids=true, to_apply=%region_7.8 | all-reduce | flops 16 | bytes 128 | tf_op jit(solution)/shard_map/psum | solution.py:110
  53.6 0.8 multiply_convert_fusion
  54.5 4.6 %all_gather.3 = bf16[16,2048]{1,0:T(8,128)(2,1)S(1)} all-gather(bf16[16,1024]{1,0:T(8,128)(2,1)S(1)} %multiply_convert_fusion), channel_id=1, replica_groups=mesh['ep'=16,'tp'=2] {'tp'}, dimensions={1}, use_global_device_ids=true | all-gather | bytes 98304 | tf_op jit(solution)/shard_map/all_gather | solution.py:114
  59.0 1.3 convolution_convert_fusion.1
  60.3 1.3 all_to_all.23
  61.6 30.2 %all_to_all.33 = bf16[16,12,2048]{2,1,0:T(8,128)(2,1)S(1)} all-to-all(bf16[16,12,2048]{2,1,0:T(8,128)(2,1)S(1)} %all_to_all.23), channel_id=1, replica_groups=mesh['ep'=16,'tp'=2] {'ep'}, dimensions={0} | all-to-all | bytes 1572864 | tf_op jit(solution)/shard_map/all_to_all | solution.py:140
  91.8 0.7 fusion.8
  92.5 0.9 copy-done.14
  93.4 0.7 fusion.22
  94.2 0.6 fusion.2
  94.8 0.5 copy.71
  95.3 1.1 convert_element_type.102
  96.5 11.9 %all_to_all.34 = bf16[16,16,128]{2,0,1:T(8,128)(2,1)S(1)} all-to-all(bf16[16,16,128]{2,0,1:T(8,128)(2,1)S(1)} %copy_bitcast_fusion), channel_id=1, replica_groups=mesh['ep'=16,'tp'=2] {'ep'}, dimensions={1} | all-to-all | bytes 131072 | tf_op jit(solution)/shard_map/all_to_all | solution.py:154
  108.3 1.0 fusion.47
  109.6 3.9 %reduce-scatter.7.cloned.1.call-done = bf16[192,1024]{1,0:T(8,128)(2,1)} async-done(((bf16[192,2048]{1,0:T(8,128)(2,1)}), bf16[192,1024]{1,0:T(8,128)(2,1)}) %reduce-scatter.7.cloned.1.call-update) | async-done | bytes 393232 | tf_op jit(solution)/shard_map/reduce_scatter | solution.py:167
  113.5 1.9 reshape.125
  115.4 5.8 %all-to-all-start.1 = ((bf16[16,12,1024]{2,1,0:T(8,128)(2,1)}), bf16[16,12,1024]{2,1,0:T(8,128)(2,1)S(1)}, u32[]{:S(2)}, u32[]{:S(2)}) async-start(bf16[16,12,1024]{2,1,0:T(8,128)(2,1)} %reshape.125), calls=%async_computation.3 | async-start | bytes 1048576 | tf_op jit(solution)/shard_map/all_to_all | solution.py:177
  121.7 0.7 reshape.127
  122.5 50.9 %reduce-scatter.9.cloned.1.call-done = f32[16,512]{1,0:T(8,128)} async-done(((f32[256,512]{1,0:T(8,128)}), f32[16,512]{1,0:T(8,128)}) %reduce-scatter.9.cloned.1.call-update) | async-done | bytes 32784 | tf_op jit(solution)/shard_map/reduce_scatter | solution.py:156
  173.4 2.1 %convolution_convert_fusion.2 = bf16[16,2048]{1,0:T(8,128)(2,1)} fusion(bf16[256,2048]{1,0:T(8,128)(2,1)} %param.36, f32[16,512]{1,0:T(8,128)} %reduce-scatter.9.cloned.1.call-done), kind=kOutput, calls=%fused_computation.7 | convolution fusion | flops 16834560 | bytes 1146880 | tf_op jit(solution)/shard_map/dot_general | solution.py:165
  175.8 8.9 %reduce-scatter.11.cloned.1.call-done = bf16[16,1024]{1,0:T(8,128)(2,1)} async-done(((bf16[16,2048]{1,0:T(8,128)(2,1)}), bf16[16,1024]{1,0:T(8,128)(2,1)}) %reduce-scatter.11.cloned.1.call-update) | async-done | bytes 32784 | tf_op jit(solution)/shard_map/reduce_scatter | solution.py:170
  184.7 1.6 fusion.26
  (70 shorter events, 3.1 us)
Async XLA Ops:
  7.2 87.0 %copy-start = (bf16[1,512,2048]{2,1,0:T(8,128)(2,1)S(1)}, bf16[1,512,2048]{2,1,0:T(8,128)(2,1)}, u32[]{:S(2)}) copy-start(bf16[1,512,2048]{2,1,0:T(8,128)(2,1)} %param.33) | copy-start | bytes 6291460
  7.2 40.6 %reduce-scatter.5.cloned.1.call-start = ((), (), s32[]{:S(2)}) async-start(), calls=%async_computation.7 | async-start | bytes 98304 | tf_op jit(solution)/shard_map/reduce_scatter | solution.py:105
  10.5 12.3 %copy-start.12 = (s32[16]{0:T(128)S(1)}, s32[16]{0:T(128)}, u32[]{:S(2)}) copy-start(s32[16]{0:T(128)} %param.20) | copy-start | bytes 196
  10.5 12.4 %copy-start.15 = (f32[8]{0:T(128)S(1)}, f32[8]{0:T(128)}, u32[]{:S(2)}) copy-start(f32[8]{0:T(128)} %param.26) | copy-start | bytes 100
  32.2 2.8 %copy-start.8 = (s32[16,6]{0,1:T(8,128)S(1)}, s32[16,6]{0,1:T(8,128)}, u32[]{:S(2)}) copy-start(s32[16,6]{0,1:T(8,128)} %param.29) | copy-start | bytes 1156
  32.2 3.3 %copy-start.11 = (f32[2048]{0:T(1024)S(1)}, f32[2048]{0:T(1024)}, u32[]{:S(2)}) copy-start(f32[2048]{0:T(1024)} %param.28) | copy-start | bytes 24580
  32.2 15.6 %copy-start.1 = (bf16[16,2048]{1,0:T(8,128)(2,1)S(1)}, bf16[16,2048]{1,0:T(8,128)(2,1)}, u32[]{:S(2)}) copy-start(bf16[16,2048]{1,0:T(8,128)(2,1)} %param.19) | copy-start | bytes 196612
  34.9 78.6 %reduce-scatter.7.cloned.1.call-start = ((), (), s32[]{:S(2)}) async-start(), calls=%async_computation.8 | async-start | bytes 1179648 | tf_op jit(solution)/shard_map/reduce_scatter | solution.py:167
  61.6 30.3 %copy-start.13 = (bf16[1,2048,512]{2,1,0:T(8,128)(2,1)S(1)}, bf16[1,2048,512]{2,1,0:T(8,128)(2,1)}, u32[]{:S(2)}) copy-start(bf16[1,2048,512]{2,1,0:T(8,128)(2,1)} %param.31) | copy-start | bytes 6291460
  91.8 1.6 copy-start.14
  94.8 13.5 %copy-start.6 = (bf16[128,256]{1,0:T(8,128)(2,1)S(1)}, bf16[128,256]{1,0:T(8,128)(2,1)}, u32[]{:S(2)}) copy-start(bf16[128,256]{1,0:T(8,128)(2,1)} %param.35) | copy-start | bytes 196612
  94.8 13.5 %copy-start.7 = (bf16[128,256]{1,0:T(8,128)(2,1)S(1)}, bf16[128,256]{1,0:T(8,128)(2,1)}, u32[]{:S(2)}) copy-start(bf16[128,256]{1,0:T(8,128)(2,1)} %param.34) | copy-start | bytes 196612
  95.3 14.1 %copy-start.5 = (f32[2048]{0:T(1024)S(1)}, f32[2048]{0:T(1024)}, u32[]{:S(2)}) copy-start(f32[2048]{0:T(1024)} %param.22) | copy-start | bytes 24580
  96.4 13.0 %copy-start.2 = (bf16[2048,128]{1,0:T(8,128)(2,1)S(1)}, bf16[2048,128]{1,0:T(8,128)(2,1)}, u32[]{:S(2)}) copy-start(bf16[2048,128]{1,0:T(8,128)(2,1)} %param.24) | copy-start | bytes 1572868
  96.4 24.8 %copy-start.3 = (bf16[2048,128]{1,0:T(8,128)(2,1)S(1)}, bf16[2048,128]{1,0:T(8,128)(2,1)}, u32[]{:S(2)}) copy-start(bf16[2048,128]{1,0:T(8,128)(2,1)} %param.25) | copy-start | bytes 1572868
  96.4 77.0 %reduce-scatter.9.cloned.1.call-start = ((), (), s32[]{:S(2)}) async-start(), calls=%async_computation.9 | async-start | bytes 557056 | tf_op jit(solution)/shard_map/reduce_scatter | solution.py:156
  108.3 13.1 %copy-start.9 = (bf16[2048]{0:T(1024)(128)(2,1)S(1)}, bf16[2048]{0:T(1024)(128)(2,1)}, u32[]{:S(2)}) copy-start(bf16[2048]{0:T(1024)(128)(2,1)} %param.37) | copy-start | bytes 12292
  108.3 14.0 %copy-start.10 = (f32[16,6]{0,1:T(8,128)S(1)}, f32[16,6]{0,1:T(8,128)}, u32[]{:S(2)}) copy-start(f32[16,6]{0,1:T(8,128)} %param.30) | copy-start | bytes 1156
  115.4 69.3 %copy-start.4 = (bf16[16,1024]{1,0:T(8,128)(2,1)S(1)}, bf16[16,1024]{1,0:T(8,128)(2,1)}, u32[]{:S(2)}) copy-start(bf16[16,1024]{1,0:T(8,128)(2,1)} %reduce-scatter.5.cloned.1.call-done) | copy-start | bytes 98308
  115.4 60.3 %all-to-all-start.1 = ((bf16[16,12,1024]{2,1,0:T(8,128)(2,1)}), bf16[16,12,1024]{2,1,0:T(8,128)(2,1)S(1)}, u32[]{:S(2)}, u32[]{:S(2)}) async-start(bf16[16,12,1024]{2,1,0:T(8,128)(2,1)} %reshape.125), calls=%async_computation.3 | async-start | bytes 1048576 | tf_op jit(solution)/shard_map/all_to_all | solution.py:177
  121.1 63.5 %reduce-scatter.11.cloned.1.call-start = ((), (), s32[]{:S(2)}) async-start(), calls=%async_computation.10 | async-start | bytes 98304 | tf_op jit(solution)/shard_map/reduce_scatter | solution.py:170
Sparse Core Ops, SparseCore 0:
  35.0 12.7 reduce-scatter.4
  96.5 16.9 reduce-scatter.6
  117.0 56.2 reduce-scatter.8
  175.6 9.0 reduce-scatter.10
where the time goes:
time: 194 us; the launch traced here: 193 us
  waiting for transfers between devices  76 us (39%)
  blocking collectives  51.6 us (27%)
  matrix products  21.9 us (11%)
  local copies, waits for them, and re-layouts  20 us (10%)
  between operations  14.1 us (7%)
  starting transfers between devices  5.93 us (3%)
  other arithmetic  3.41 us (2%)
    reduce_scatter x1, waiting for transfers between devices, shards(): lax.psum_scatter(jnp.dot(column_rows, joined_weights, preferred_element_t...  50.9 us
    all_to_all x1, blocking collectives, shards(): lax.all_to_all(sent_rows, 'ep', split_axis=0, concat_axis=0, tiled=True)  30.2 us
    unnamed x35, local copies, waits for them, and re-layouts  13.4 us
    reduce_scatter x1, waiting for transfers between devices, shards(): lax.psum_scatter(attn_term.astype(jnp.bfloat16), 'tp', scatter_dimension=...  12.2 us
    all_to_all x1, blocking collectives, shards(): lax.all_to_all(normed_mix, 'ep', split_axis=1, concat_axis=0, tiled=True)  11.9 us
    reduce_scatter x1, waiting for transfers between devices, shards(): lax.psum_scatter(shared_term.astype(jnp.bfloat16), 'tp', scatter_dimensio...  8.93 us
    all_to_all x1, starting transfers between devices, shards(): lax.all_to_all(expert_out, 'ep', split_axis=0, concat_axis=0, tiled=True)  5.77 us
    psum x1, blocking collectives, shards(): stat_total = lax.psum(jnp.sum(residual * residual, axis=1), 'tp')  4.93 us
  transfers between devices with their start and end apart: 5, of which 4 were waited for; matrix products, arithmetic and copies ran while one was open for 4% of the time, Pallas kernels for 0%

commit v1 on v0

v1 whole, which is shorter than its diff:
```python
import functools

import jax
import jax.numpy as jnp
from jax import lax
from jax.experimental import pallas as pl
from jax.experimental.pallas import tpu as pltpu
from jax.sharding import PartitionSpec as P

HEAD_DIM = 64
LANES = 128
epsilon = 1e-06
MESH = pl.DeviceIdType.MESH
F32 = jnp.float32
BF16 = jnp.bfloat16


def rms_scale(rows_in, gain_row):
    values_f = rows_in.astype(F32)
    return (
        values_f
        * lax.rsqrt(jnp.mean(values_f * values_f, axis=-1, keepdims=True) + epsilon)
        * gain_row
    )


def attend_kernel(groups, query_ref, span_ref, bias_ref, cache_ref, out_ref, held, logits, sems):
    seqs, heads, _ = query_ref.shape
    length = cache_ref.shape[1]
    width = 256
    count = length // width
    copies = []
    for s in range(seqs):
        copy = pltpu.make_async_copy(cache_ref.at[s], held.at[s], sems.at[s])
        copy.start()
        copies.append(copy)
    table = (
        lax.broadcasted_iota(jnp.int32, (width, width), 0)
        >= lax.broadcasted_iota(jnp.int32, (width, width), 1)
    ).astype(F32)
    per_group = seqs // groups
    rows = per_group * heads
    for g in range(groups):
        first = g * per_group
        for s in range(first, first + per_group):
            copies[s].wait()
            logits[s * heads : (s + 1) * heads, :] = lax.dot_general(
                query_ref[s], held[s], (((1,), (1,)), ((), ())), preferred_element_type=F32
            )
        span = slice(first * heads, first * heads + rows)
        limit = span_ref[span, :]
        offset = bias_ref[span, :]
        carried = jnp.zeros((rows, 1), F32)
        for b in range(count - 1, -1, -1):
            cols = slice(b * width, (b + 1) * width)
            z = logits[span, cols] * HEAD_DIM ** (-0.5) + offset
            position = lax.broadcasted_iota(jnp.int32, (rows, width), 1) + b * width
            usable = position < limit
            soft = jnp.where(usable, jnp.maximum(z, 0.0) + jnp.log1p(jnp.exp(-jnp.abs(z))), 0.0)
            behind = jnp.dot(soft, table, precision=lax.Precision.HIGHEST, preferred_element_type=F32)
            weight = jnp.where(usable, jnp.exp(z - behind - carried), 0.0)
            carried = carried + jnp.sum(soft, axis=1, keepdims=True)
            logits[span, cols] = weight
        for s in range(first, first + per_group):
            out_ref[s] = jnp.dot(
                logits[s * heads : (s + 1) * heads, :].astype(BF16),
                held[s],
                preferred_element_type=F32,
            )


def attend(query_grid, lengths, bias, cache):
    seqs, heads, lanes = query_grid.shape
    length = cache.shape[1]
    span_rows = jnp.repeat(lengths, heads).reshape(seqs * heads, 1)
    bias_rows = jnp.tile(bias, seqs).reshape(seqs * heads, 1)
    vmem = pl.BlockSpec(memory_space=pltpu.VMEM)
    return pl.pallas_call(
        functools.partial(attend_kernel, 2),
        out_shape=jax.ShapeDtypeStruct((seqs, heads, lanes), F32),
        in_specs=[vmem, vmem, vmem, pl.BlockSpec(memory_space=pl.ANY)],
        out_specs=vmem,
        scratch_shapes=[
            pltpu.VMEM((seqs, length, lanes), BF16),
            pltpu.VMEM((seqs * heads, length), F32),
            pltpu.SemaphoreType.DMA((seqs,)),
        ],
        compiler_params=pltpu.CompilerParams(vmem_limit_bytes=60 * 2**20),
    )(query_grid, span_rows, bias_rows, cache)


def mix_kernel(
    ranks_ep,
    ranks_tp,
    partial_ref,
    tokens_ref,
    gain_ref,
    vector_ref,
    route_ref,
    sgate_ref,
    sup_ref,
    sdown_hbm,
    gate_hbm,
    up_hbm,
    down_hbm,
    out_ref,
    attn_in,
    residual_ref,
    gathered,
    hidden_ref,
    terms,
    terms_in,
    shared,
    shared_in,
    last,
    last_in,
    gate_w,
    up_w,
    down_w,
    sdown_w,
    load_sem,
    tp_send,
    tp_recv,
    ag_send,
    ag_recv,
    rs_send,
    rs_recv,
    sh_send,
    sh_recv,
    out_send,
    out_recv,
):
    me = lax.axis_index("ep")
    my_tp = lax.axis_index("tp")
    row_count, width = tokens_ref.shape
    experts = gate_w.shape[0]
    bits = ranks_ep.bit_length() - 1
    weights = [ranks_ep >> (i + 1) for i in range(bits)]
    mine = [(me // w) % 2 for w in weights]
    partner = [me + (1 - 2 * mine[i]) * weights[i] for i in range(bits)]
    all_rows = ranks_ep * row_count

    loads = []
    for i, (source, target) in enumerate(
        ((gate_hbm, gate_w), (up_hbm, up_w), (down_hbm, down_w), (sdown_hbm, sdown_w))
    ):
        load = pltpu.make_async_copy(source, target, load_sem.at[i])
        load.start()
        loads.append(load)

    barrier = pltpu.get_barrier_semaphore()
    for i in range(bits):
        pl.semaphore_signal(barrier, inc=1, device_id={"ep": partner[i]}, device_id_type=MESH)
    for step in range(1, ranks_tp):
        pl.semaphore_signal(
            barrier, inc=1, device_id={"tp": lax.rem(my_tp + step, ranks_tp)}, device_id_type=MESH
        )
    pl.semaphore_wait(barrier, bits + ranks_tp - 1)

    swaps = []
    for step in range(1, ranks_tp):
        swap = pltpu.make_async_remote_copy(
            src_ref=partial_ref,
            dst_ref=attn_in.at[step - 1],
            send_sem=tp_send.at[step - 1],
            recv_sem=tp_recv.at[step - 1],
            device_id={"tp": lax.rem(my_tp + step, ranks_tp)},
            device_id_type=MESH,
        )
        swap.start()
        swaps.append(swap)
    residual = partial_ref[...].astype(F32)
    for step in range(1, ranks_tp):
        swaps[step - 1].wait()
        residual = residual + attn_in[step - 1].astype(F32)
    residual = residual + tokens_ref[...].astype(F32)
    residual_ref[...] = residual
    normed = (
        residual
        * lax.rsqrt(jnp.mean(residual * residual, axis=-1, keepdims=True) + epsilon)
        * gain_ref[...]
    ).astype(BF16)
    gathered[(*mine, slice(None), pl.ds(0, width))] = normed
    gathered[(*mine, slice(None), pl.ds(width, route_ref.shape[1]))] = route_ref[...]
    mix_gate = jax.nn.sigmoid(
        jnp.sum(normed.astype(F32) * vector_ref[...].astype(F32), axis=1, keepdims=True)
    )

    core = bits - 1
    near = max(bits - 2, 0)
    others = [i for i in range(bits) if i not in (core, near)]
    orders = ([*others, near, core], [near, *others, core])
    orders = tuple(list(dict.fromkeys(order)) for order in orders)
    half = width // 2
    spans = (pl.ds(0, half), pl.ds(half, gathered.shape[-1] - half))

    def region(done):
        return tuple(slice(None) if i in done else mine[i] for i in range(bits))

    pulls = {}
    for turn in range(bits):
        for s in range(2):
            if turn > 0:
                pulls[s, turn - 1].wait_recv()
            axis = orders[s][turn]
            where = (*region(orders[s][:turn]), slice(None), spans[s])
            pull = pltpu.make_async_remote_copy(
                src_ref=gathered.at[where],
                dst_ref=gathered.at[where],
                send_sem=ag_send.at[s, turn],
                recv_sem=ag_recv.at[s, turn],
                device_id={"ep": partner[axis]},
                device_id_type=MESH,
            )
            pull.start()
            pulls[s, turn] = pull
    for s in range(2):
        pulls[s, bits - 1].wait_recv()
    for pull in pulls.values():
        pull.wait_send()

    def reduce_at(fixed, axis, other):
        return tuple(
            (1 - mine[i] if other else mine[i]) if i == axis else mine[i] if i in fixed else slice(None)
            for i in range(bits)
        )

    def push(source, landing, order, turn, cols, send, recv):
        axis = order[turn]
        copy = pltpu.make_async_remote_copy(
            src_ref=source.at[(*reduce_at(order[:turn], axis, True), slice(None), cols)],
            dst_ref=landing.at[(*reduce_at(order[:turn], axis, False), slice(None), cols)],
            send_sem=send,
            recv_sem=recv,
            device_id={"ep": partner[axis]},
            device_id_type=MESH,
        )
        copy.start()
        return copy

    def fold(source, landing, order, turn, cols):
        axis = order[turn]
        own = (*reduce_at(order[:turn], axis, False), slice(None), cols)
        came = (*reduce_at(order[:turn], axis, True), slice(None), cols)
        return source[own].astype(F32) + landing[came].astype(F32), own

    shared_cols = sgate_ref.shape[1]
    depth = sgate_ref.shape[0]
    feature_at = pl.ds(pl.multiple_of(me * (width // ranks_ep) // depth * depth, depth), depth)
    everyone = (slice(None),) * bits
    features = gathered[(*everyone, slice(None), feature_at)].reshape(all_rows, depth)
    grid = tuple(2 for _ in range(bits)) + (row_count,)
    for i, part in enumerate((sgate_ref, sup_ref)):
        shared[(*everyone, slice(None), pl.ds(i * shared_cols, shared_cols))] = (
            jnp.dot(features, part[...], preferred_element_type=F32)
            .astype(BF16)
            .reshape(*grid, shared_cols)
        )
    shared_order = orders[0][::-1]
    shared_span = pl.ds(0, 2 * shared_cols)
    state = {"turn": -1, "copies": []}

    def advance_shared():
        turn = state["turn"]
        total = None
        if turn >= 0:
            state["copies"][turn].wait_recv()
            total, own = fold(shared, shared_in, shared_order, turn, shared_span)
            if turn < bits - 1:
                shared[own] = total.astype(BF16)
        if turn < bits - 1:
            turn = turn + 1
            state["turn"] = turn
            state["copies"].append(
                push(
                    shared,
                    shared_in,
                    shared_order,
                    turn,
                    shared_span,
                    sh_send.at[turn],
                    sh_recv.at[turn],
                )
            )
        return total

    advance_shared()
    rows = gathered[(*everyone, slice(None), pl.ds(0, width))].reshape(all_rows, width)
    route_cols = gathered[
        (*everyone, slice(None), pl.ds(width, route_ref.shape[1]))
    ].reshape(all_rows, route_ref.shape[1])
    lane = lax.broadcasted_iota(jnp.int32, route_cols.shape, 1)
    stride = route_ref.shape[1] // 2
    route_cols = route_cols.astype(F32)
    loads[0].wait()
    loads[1].wait()
    scales = []
    for j in range(experts):
        wanted = me * experts + j
        chosen = jnp.where((lane == wanted) | (lane == wanted + stride), route_cols, 0.0)
        scales.append(jnp.sum(chosen, axis=1, keepdims=True))
        gate_val = jnp.dot(rows, gate_w[j], preferred_element_type=F32)
        up_val = jnp.dot(rows, up_w[j], preferred_element_type=F32)
        hidden_ref[j] = (gate_val * jax.nn.sigmoid(gate_val) * up_val).astype(BF16)
    total = advance_shared()
    loads[2].wait()
    loads[3].wait()
    reduce_orders = tuple(order[::-1] for order in ([*orders[0]], [*orders[1]]))
    reduce_spans = (pl.ds(0, half), pl.ds(half, width - half))
    sums = {}
    for s in range(2):
        term = jnp.zeros((all_rows, half), F32)
        for j in range(experts):
            term = term + scales[j] * jnp.dot(
                hidden_ref[j], down_w[j, :, s * half : (s + 1) * half], preferred_element_type=F32
            )
        terms[(*everyone, slice(None), reduce_spans[s])] = term.astype(BF16).reshape(*grid, half)
        sums[s, 0] = push(
            terms, terms_in, reduce_orders[s], 0, reduce_spans[s], rs_send.at[s, 0], rs_recv.at[s, 0]
        )
        total = advance_shared() if state["turn"] < bits - 1 else total
    pieces = []
    for turn in range(bits):
        for s in range(2):
            sums[s, turn].wait_recv()
            value, own = fold(terms, terms_in, reduce_orders[s], turn, reduce_spans[s])
            if turn < bits - 1:
                terms[own] = value.astype(BF16)
                sums[s, turn + 1] = push(
                    terms,
                    terms_in,
                    reduce_orders[s],
                    turn + 1,
                    reduce_spans[s],
                    rs_send.at[s, turn + 1],
                    rs_recv.at[s, turn + 1],
                )
            else:
                pieces.append(value)
        if turn == 0:
            while state["turn"] < bits - 1:
                advance_shared()
            total = advance_shared()
            gate_sum = total[:, :shared_cols]
            up_sum = total[:, shared_cols:]
            shared_hidden = (gate_sum * jax.nn.sigmoid(gate_sum) * up_sum).astype(BF16)
            shared_term = mix_gate * jnp.dot(
                shared_hidden, sdown_w[...], preferred_element_type=F32
            )
    for copy in (*sums.values(), *state["copies"]):
        copy.wait_send()
    for s in range(2):
        cols = slice(s * half, (s + 1) * half)
        last[:, cols] = (pieces[s] + shared_term[:, cols]).astype(BF16)
    quarter = width // ranks_tp

    def quarter_of(index):
        return pl.ds(pl.multiple_of(index * quarter, quarter), quarter)

    ends = []
    for step in range(1, ranks_tp):
        goal = lax.rem(my_tp + step, ranks_tp)
        end = pltpu.make_async_remote_copy(
            src_ref=last.at[:, quarter_of(goal)],
            dst_ref=last_in.at[step - 1],
            send_sem=out_send.at[step - 1],
            recv_sem=out_recv.at[step - 1],
            device_id={"tp": goal},
            device_id_type=MESH,
        )
        end.start()
        ends.append(end)
    result = residual_ref[:, quarter_of(my_tp)] + last[:, quarter_of(my_tp)].astype(F32)
    for step in range(1, ranks_tp):
        ends[step - 1].wait()
        result = result + last_in[step - 1].astype(F32)
    out_ref[...] = result.astype(BF16)


def mix(
    ranks_ep,
    ranks_tp,
    attn_term,
    tokens,
    ffn_gain,
    gate_vector,
    route_table,
    shared_gate,
    shared_up,
    shared_down,
    expert_gate,
    expert_up,
    expert_down,
):
    row_count, width = tokens.shape
    bits = ranks_ep.bit_length() - 1
    grid = (2,) * bits + (row_count,)
    experts, _, hidden = expert_gate.shape
    shared_cols = shared_gate.shape[1]
    quarter = width // ranks_tp
    swaps = max(ranks_tp - 1, 1)
    vmem = pl.BlockSpec(memory_space=pltpu.VMEM)
    anywhere = pl.BlockSpec(memory_space=pl.ANY)
    dma = pltpu.SemaphoreType.DMA
    return pl.pallas_call(
        functools.partial(mix_kernel, ranks_ep, ranks_tp),
        out_shape=jax.ShapeDtypeStruct((row_count, quarter), BF16),
        in_specs=[vmem] * 7 + [anywhere] * 4,
        out_specs=vmem,
        scratch_shapes=[
            pltpu.VMEM((swaps, row_count, width), BF16),
            pltpu.VMEM((row_count, width), F32),
            pltpu.VMEM((*grid, width + route_table.shape[1]), BF16),
            pltpu.VMEM((experts, ranks_ep * row_count, hidden), BF16),
            pltpu.VMEM((*grid, width), BF16),
            pltpu.VMEM((*grid, width), BF16),
            pltpu.VMEM((*grid, 2 * shared_cols), BF16),
            pltpu.VMEM((*grid, 2 * shared_cols), BF16),
            pltpu.VMEM((row_count, width), BF16),
            pltpu.VMEM((swaps, row_count, quarter), BF16),
            pltpu.VMEM(expert_gate.shape, BF16),
            pltpu.VMEM(expert_up.shape, BF16),
            pltpu.VMEM(expert_down.shape, BF16),
            pltpu.VMEM(shared_down.shape, BF16),
            dma((4,)),
            dma((swaps,)),
            dma((swaps,)),
            dma((2, bits)),
            dma((2, bits)),
            dma((2, bits)),
            dma((2, bits)),
            dma((bits,)),
            dma((bits,)),
            dma((swaps,)),
            dma((swaps,)),
        ],
        compiler_params=pltpu.CompilerParams(
            collective_id=0, has_side_effects=True, vmem_limit_bytes=60 * 2**20
        ),
    )(
        attn_term,
        tokens,
        ffn_gain.reshape(1, width),
        gate_vector.reshape(1, width),
        route_table,
        shared_gate,
        shared_up,
        shared_down,
        expert_gate,
        expert_up,
        expert_down,
    )


def shards(
    ranks_ep,
    ranks_tp,
    tokens,
    lengths,
    cache,
    attn_gain,
    query_weight,
    key_weight,
    value_weight,
    stick_bias,
    out_weight,
    ffn_gain,
    routes,
    route_weights,
    expert_gate,
    expert_up,
    expert_down,
    shared_gate,
    shared_up,
    shared_down,
    gate_vector,
):
    row_count = tokens.shape[0]
    normed = rms_scale(tokens, attn_gain).astype(BF16)
    queries = jnp.dot(normed, query_weight, preferred_element_type=F32).astype(BF16)
    key_rows = jnp.dot(normed, key_weight, preferred_element_type=F32).astype(BF16)
    value_rows = jnp.dot(normed, value_weight, preferred_element_type=F32).astype(BF16)
    heads = key_weight.shape[1] // HEAD_DIM
    new_kv = jnp.stack(
        [
            key_rows.reshape(row_count, heads, HEAD_DIM),
            value_rows.reshape(row_count, heads, HEAD_DIM),
        ],
        axis=2,
    ).reshape(row_count, heads * 2 * HEAD_DIM)
    group = queries.shape[1] // HEAD_DIM // heads
    same = jnp.eye(heads, dtype=jnp.bool_)
    spread = jnp.where(
        same[None, :, None, :, None],
        queries.reshape(row_count, heads, group, 1, HEAD_DIM),
        jnp.zeros((), BF16),
    )
    spread = jnp.pad(spread, ((0, 0),) * 4 + ((0, HEAD_DIM),))
    query_grid = spread.reshape(row_count, heads * group, heads * 2 * HEAD_DIM)
    mixed = attend(query_grid, lengths, stick_bias, cache)
    mixed = mixed.reshape(row_count, heads, group, heads, 2 * HEAD_DIM)[..., HEAD_DIM:]
    heads_out = jnp.sum(jnp.where(same[None, :, None, :, None], mixed, 0.0), axis=3).astype(BF16)
    attn_term = jnp.dot(
        heads_out.reshape(row_count, -1), out_weight, preferred_element_type=F32
    ).astype(BF16)
    experts_all = ranks_ep * expert_gate.shape[0]
    stride = -(-2 * experts_all // LANES) * LANES // 2
    named = routes[:, :, None] == lax.broadcasted_iota(jnp.int32, (1, 1, stride), 2)
    dense = jnp.sum(jnp.where(named, route_weights[:, :, None], 0.0), axis=1)
    high = lax.reduce_precision(dense, 8, 7)
    route_table = jnp.concatenate([high, dense - high], axis=1).astype(BF16)
    depth = shared_gate.shape[0]
    if depth % LANES:
        slot = lax.axis_index("ep") * depth % LANES
        wide = jnp.zeros((LANES, shared_gate.shape[1]), BF16)
        shared_gate = lax.dynamic_update_slice_in_dim(wide, shared_gate, slot, 0)
        shared_up = lax.dynamic_update_slice_in_dim(wide, shared_up, slot, 0)
    layer_out = mix(
        ranks_ep,
        ranks_tp,
        attn_term,
        tokens,
        ffn_gain,
        gate_vector,
        route_table,
        shared_gate,
        shared_up,
        shared_down,
        expert_gate,
        expert_up,
        expert_down,
    )
    return (layer_out, new_kv)


def solution(mesh):
    placed = (
        P("ep", None),
        P("ep"),
        P("ep", None, "tp"),
        P(),
        P(None, "tp"),
        P(None, "tp"),
        P(None, "tp"),
        P("tp"),
        P("tp", None),
        P(),
        P("ep", None),
        P("ep", None),
        P("ep", None, "tp"),
        P("ep", None, "tp"),
        P("ep", "tp", None),
        P("ep", "tp"),
        P("ep", "tp"),
        P("tp", None),
        P(),
    )
    return jax.shard_map(
        functools.partial(shards, mesh.shape["ep"], mesh.shape["tp"]),
        mesh=mesh,
        in_specs=placed,
        out_specs=(P("ep", "tp"), P("ep", "tp")),
        check_vma=False,
    )
```

time: 194 us -> 69.7 us (0.36)
  waiting for transfers between devices: 76 us -> 0 us
  Pallas kernels: 0 us -> 56.4 us
  blocking collectives: 51.6 us -> 0 us
  matrix products: 21.9 us -> 3.56 us
  local copies, waits for them, and re-layouts: 20 us -> 6.32 us
  between operations: 14.1 us -> 0.8 us
  starting transfers between devices: 5.93 us -> 0 us
    reduce_scatter x4 -> x0, waiting for transfers between devices: 75.9 us -> none  [the longest x1 50.9 us: shards(): lax.psum_scatter(jnp.dot(column_rows, joined_weights, preferred_element_t...]
    pallas_call x0 -> x2, Pallas kernels: none -> 56.4 us  [the longest x1 47.1 us: mix(): pl.pallas_call(functools.partial(mix_kernel, ranks_ep, ranks_tp), out_sha...]
    all_to_all x2 -> x0, blocking collectives: 42.1 us -> none  [the longest x1 30.2 us: shards(): lax.all_to_all(sent_rows, 'ep', split_axis=0, concat_axis=0, tiled=True)]
    dot_general x16 -> x3, matrix products: 19.3 us -> 2.55 us  [the longest x1 2.07 us: shards(): jnp.dot(normed, query_weight, preferred_element_type=F32).astype(BF16)]
    unnamed x35 -> x21, local copies, waits for them, and re-layouts: 13.4 us -> 1.43 us
    all_to_all x1 -> x0, starting transfers between devices: 5.77 us -> none  [shards(): lax.all_to_all(expert_out, 'ep', split_axis=0, concat_axis=0, tiled=True)]
    psum x1 -> x0, blocking collectives: 4.93 us -> none  [shards(): stat_total = lax.psum(jnp.sum(residual * residual, axis=1), 'tp')]
    all_gather x1 -> x0, blocking collectives: 4.57 us -> none  [shards(): normed_mix = lax.all_gather(normed_part, 'tp', axis=1, tiled=True)]
  transfers between devices with their start and end apart: 5 -> 0, of which waited for: 4 -> 0; matrix products, arithmetic and copies ran while one was open for 4% -> 0% of each run, Pallas kernels for 0% -> 0%
where the time goes in v1:
time: 69.7 us; the launch traced here: 69.4 us
  Pallas kernels  56.4 us (81%)
  local copies, waits for them, and re-layouts  6.32 us (9%)
  matrix products  3.56 us (5%)
  other arithmetic  2.33 us (3%)
  between operations  0.8 us (1%)
    pallas_call x1, Pallas kernels, mix(): pl.pallas_call(functools.partial(mix_kernel, ranks_ep, ranks_tp), out_sha...  47.1 us
    pallas_call x1, Pallas kernels, attend(): pl.pallas_call(functools.partial(attend_kernel, 2), out_shape=jax.ShapeDt...  9.26 us
    dot_general x1, matrix products, shards(): jnp.dot(normed, query_weight, preferred_element_type=F32).astype(BF16)  2.07 us
    unnamed x21, local copies, waits for them, and re-layouts  1.43 us

profile of v1, /device:TPU:0, one launch (start us, length us, event | category | flops | bytes accessed | tf_op | source)
XLA Modules:
  0.0 69.4 jit_solution(11135063207899947132)
XLA Ops:
  0.6 0.0 copy-start
  0.6 0.0 copy-start.8
  0.7 0.0 copy-start.9
  0.7 1.1 %fusion = f32[16]{0:T(128)S(1)} fusion(bf16[16,2048]{1,0:T(8,128)(2,1)} %tokens_ref.1), kind=kLoop, calls=%fused_computation.6 | loop fusion | flops 98288 | bytes 65600 | tf_op jit(solution)/shard_map/reduce_sum | solution.py:22
  1.8 2.1 %convolution_convert_fusion.1 = bf16[16,512]{1,0:T(8,128)(2,1)S(1)} fusion(bf16[2048,512]{1,0:T(8,128)(2,1)} %param.23, bf16[16,2048]{1,0:T(8,128)(2,1)} %tokens_ref.1, f32[2048]{0:T(1024)} %param.22, f32[16]{0:T(128)S(1)} %add_rsqrt_fusion), kind=kOutput, calls=%fused_computation.1 | convolution fusion | flops 33693696 | bytes 2187328 | tf_op jit(solution)/shard_map/dot_general | solution.py:480
  3.9 0.1 broadcast_in_dim.56
  4.0 0.1 broadcast_select_fusion
  4.1 0.1 pad.4
  4.2 0.7 reshape.43.query_ref
  4.9 0.0 copy-done.8
  4.9 0.1 broadcast_in_dim.59
  4.9 0.7 %reshape_reshape.4.span_ref = s32[128,1]{1,0:T(8,128)} reshape(s32[16,8]{1,0:T(8,128)S(1)} %broadcast_in_dim.59) | data formatting | bytes 1024 | tf_op jit(solution)/shard_map/reshape;reshape | solution.py:75
  5.6 0.7 %reshape_tile.4.bias_ref = f32[128,1]{1,0:T(8,128)} reshape(f32[16,8]{1,0:T(8,128)S(1)} %tile.2) | data formatting | bytes 1024 | tf_op jit(solution)/shard_map/reshape;tile | solution.py:76
  6.4 9.3 %shard_map.194 = f32[16,8,256]{2,1,0:T(8,128)} custom-call(bf16[16,8,256]{2,1,0:T(8,128)(2,1)} %reshape.43.query_ref, s32[128,1]{1,0:T(8,128)} %reshape_reshape.4.span_ref, f32[128,1]{1,0:T(8,128)} %reshape_tile.4.bias_ref, bf16[16,1024,256]{2,1,0:T(8,128)(2,1)} %cache_ref.1), custom_call_target="tpu_custom_call" | custom-call | tf_op jit(solution)/shard_map/pallas_call | solution.py:78
  15.6 0.0 copy-start.6
  15.6 0.0 copy-start.7
  15.6 0.0 copy-start.5
  15.7 1.0 %reshape.44 = f32[16,2,4,2,128]{4,3,2,1,0:T(2,128)S(1)} reshape(f32[16,8,256]{2,1,0:T(8,128)} %shard_map.194) | data formatting | bytes 262144 | tf_op jit(solution)/shard_map/reshape | solution.py:501
  16.6 0.3 fusion.3
  16.9 0.1 convert_element_type.32
  17.0 1.0 %convolution_convert_fusion.partial_ref = bf16[16,2048]{1,0:T(8,128)(2,1)} fusion(bf16[16,512]{1,0:T(8,128)(2,1)S(1)} %convert_element_type.32, bf16[512,2048]{1,0:T(8,128)(2,1)S(1)} %copy-done), kind=kOutput, calls=%fused_computation | convolution fusion | flops 33587200 | bytes 2179072 | tf_op jit(solution)/shard_map/dot_general | solution.py:503
  18.0 0.0 copy-done.7
  18.0 0.1 select_reduce_fusion
  18.2 0.7 pad_maximum_fusion.1.route_ref
  18.8 0.6 reshape.46.vector_ref
  19.4 47.1 %shard_map.195 = bf16[16,1024]{1,0:T(8,128)(2,1)} custom-call(bf16[16,2048]{1,0:T(8,128)(2,1)} %convolution_convert_fusion.partial_ref, bf16[16,2048]{1,0:T(8,128)(2,1)} %tokens_ref.1, f32[1,2048]{1,0:T(1,128)} %bitcast.6, bf16[1,2048]{1,0:T(2,128)(2,1)} %reshape.46.vector_ref, bf16[16,128]{1,0:T(8,128)(2,1)} %pad_maximum_fusion.1.route_ref, ...), custom_call_target="tpu_custom_call" | custom-call | tf_op jit(solution)/shard_map/pallas_call | solution.py:405
  66.6 0.2 convolution_convert_fusion.3
  66.8 0.1 stack_reshape.6
  66.9 0.2 convolution_convert_fusion.2
  67.1 0.1 stack_reshape.7
  67.3 0.7 reshape.47
  68.0 1.4 %copy.35 = bf16[16,1024]{1,0:T(8,128)(2,1)} copy(bf16[16,1024]{1,0:T(8,128)(2,1)} %shard_map.195) | data formatting | bytes 65536
  (18 shorter events, 0.1 us)
Async XLA Ops:
  0.6 16.4 %copy-start = (bf16[512,2048]{1,0:T(8,128)(2,1)S(1)}, bf16[512,2048]{1,0:T(8,128)(2,1)}, u32[]{:S(2)}) copy-start(bf16[512,2048]{1,0:T(8,128)(2,1)} %param.27) | copy-start | bytes 6291460
  0.6 4.2 %copy-start.8 = (s32[16]{0:T(128)S(1)}, s32[16]{0:T(128)}, u32[]{:S(2)}) copy-start(s32[16]{0:T(128)} %param.20) | copy-start | bytes 196
  0.7 5.0 %copy-start.9 = (f32[8]{0:T(128)S(1)}, f32[8]{0:T(128)}, u32[]{:S(2)}) copy-start(f32[8]{0:T(128)} %param.26) | copy-start | bytes 100
  15.6 2.4 %copy-start.6 = (f32[16,6]{0,1:T(8,128)S(1)}, f32[16,6]{0,1:T(8,128)}, u32[]{:S(2)}) copy-start(f32[16,6]{0,1:T(8,128)} %param.30) | copy-start | bytes 1156
  15.6 2.4 %copy-start.7 = (s32[16,6]{0,1:T(8,128)S(1)}, s32[16,6]{0,1:T(8,128)}, u32[]{:S(2)}) copy-start(s32[16,6]{0,1:T(8,128)} %param.29) | copy-start | bytes 1156
  15.6 3.2 %copy-start.5 = (bf16[2048]{0:T(1024)(128)(2,1)S(1)}, bf16[2048]{0:T(1024)(128)(2,1)}, u32[]{:S(2)}) copy-start(bf16[2048]{0:T(1024)(128)(2,1)} %param.37) | copy-start | bytes 12292
  19.4 47.1 %copy-start.1 = (bf16[16,2048]{1,0:T(8,128)(2,1)S(1)}, bf16[16,2048]{1,0:T(8,128)(2,1)}, u32[]{:S(2)}) copy-start(bf16[16,2048]{1,0:T(8,128)(2,1)} %tokens_ref.1) | copy-start | bytes 196612
  19.4 47.1 %copy-start.2 = (bf16[2048,128]{1,0:T(8,128)(2,1)S(1)}, bf16[2048,128]{1,0:T(8,128)(2,1)}, u32[]{:S(2)}) copy-start(bf16[2048,128]{1,0:T(8,128)(2,1)} %param.24) | copy-start | bytes 1572868
  19.4 47.1 %copy-start.4 = (f32[2048]{0:T(1024)S(1)}, f32[2048]{0:T(1024)}, u32[]{:S(2)}) copy-start(f32[2048]{0:T(1024)} %param.22) | copy-start | bytes 24580
  19.4 47.5 %copy-start.3 = (bf16[2048,128]{1,0:T(8,128)(2,1)S(1)}, bf16[2048,128]{1,0:T(8,128)(2,1)}, u32[]{:S(2)}) copy-start(bf16[2048,128]{1,0:T(8,128)(2,1)} %param.25) | copy-start | bytes 1572868

commit v2 on v1

v2 whole, which is shorter than its diff:
```python
import functools

import jax
import jax.numpy as jnp
from jax import lax
from jax.experimental import pallas as pl
from jax.experimental.pallas import tpu as pltpu
from jax.sharding import PartitionSpec as P

HEAD_DIM = 64
LANES = 128
epsilon = 1e-06
MESH = pl.DeviceIdType.MESH
F32 = jnp.float32
BF16 = jnp.bfloat16


def rms_scale(rows_in, gain_row):
    values_f = rows_in.astype(F32)
    return (
        values_f
        * lax.rsqrt(jnp.mean(values_f * values_f, axis=-1, keepdims=True) + epsilon)
        * gain_row
    )


def attend_kernel(groups, query_ref, span_ref, bias_ref, cache_ref, out_ref, held, logits, sems):
    seqs, heads, _ = query_ref.shape
    length = cache_ref.shape[1]
    width = 256
    count = length // width
    copies = []
    for s in range(seqs):
        copy = pltpu.make_async_copy(cache_ref.at[s], held.at[s], sems.at[s])
        copy.start()
        copies.append(copy)
    table = (
        lax.broadcasted_iota(jnp.int32, (width, width), 0)
        >= lax.broadcasted_iota(jnp.int32, (width, width), 1)
    ).astype(F32)
    per_group = seqs // groups
    rows = per_group * heads
    for g in range(groups):
        first = g * per_group
        for s in range(first, first + per_group):
            copies[s].wait()
            logits[s * heads : (s + 1) * heads, :] = lax.dot_general(
                query_ref[s], held[s], (((1,), (1,)), ((), ())), preferred_element_type=F32
            )
        span = slice(first * heads, first * heads + rows)
        row = lax.broadcasted_iota(jnp.int32, (rows, 1), 0)
        limit = jnp.zeros((rows, 1), jnp.int32)
        for s in range(per_group):
            limit = jnp.where(row // heads == s, span_ref[first + s], limit)
        offset = jnp.zeros((rows, 1), F32)
        for h in range(heads):
            offset = jnp.where(row % heads == h, bias_ref[h], offset)
        carried = jnp.zeros((rows, 1), F32)
        for b in range(count - 1, -1, -1):
            cols = slice(b * width, (b + 1) * width)
            z = logits[span, cols] * HEAD_DIM ** (-0.5) + offset
            position = lax.broadcasted_iota(jnp.int32, (rows, width), 1) + b * width
            usable = position < limit
            soft = jnp.where(usable, jnp.maximum(z, 0.0) + jnp.log1p(jnp.exp(-jnp.abs(z))), 0.0)
            behind = jnp.dot(soft, table, precision=lax.Precision.HIGHEST, preferred_element_type=F32)
            weight = jnp.where(usable, jnp.exp(z - behind - carried), 0.0)
            carried = carried + jnp.sum(soft, axis=1, keepdims=True)
            logits[span, cols] = weight
        for s in range(first, first + per_group):
            out_ref[s] = jnp.dot(
                logits[s * heads : (s + 1) * heads, :].astype(BF16),
                held[s],
                preferred_element_type=F32,
            )


def attend(query_grid, lengths, bias, cache):
    seqs, heads, lanes = query_grid.shape
    length = cache.shape[1]
    smem = pl.BlockSpec(memory_space=pltpu.SMEM)
    vmem = pl.BlockSpec(memory_space=pltpu.VMEM)
    return pl.pallas_call(
        functools.partial(attend_kernel, 2),
        out_shape=jax.ShapeDtypeStruct((seqs, heads, lanes), F32),
        in_specs=[vmem, smem, smem, pl.BlockSpec(memory_space=pl.ANY)],
        out_specs=vmem,
        scratch_shapes=[
            pltpu.VMEM((seqs, length, lanes), BF16),
            pltpu.VMEM((seqs * heads, length), F32),
            pltpu.SemaphoreType.DMA((seqs,)),
        ],
        compiler_params=pltpu.CompilerParams(vmem_limit_bytes=60 * 2**20),
    )(query_grid, lengths, bias, cache)


def reduce_rounds(own, landing, flip, zmasks, ymasks, cols, send_sem, recv_sem, sent):
    def push(block, goal, slot):
        copy = pltpu.make_async_remote_copy(
            src_ref=own.at[block, :, cols],
            dst_ref=landing.at[slot, :, cols],
            send_sem=send_sem.at[len(sent)],
            recv_sem=recv_sem.at[slot],
            device_id={"ep": flip(goal)},
            device_id_type=MESH,
        )
        copy.start()
        sent.append(copy)
        arrivals[slot] = copy

    def fold(block, slots):
        total = own[block, :, cols].astype(F32)
        for slot in slots:
            arrivals[slot].wait_recv()
            total = total + landing[slot, :, cols].astype(F32)
        return total

    arrivals = {}
    for y in (*ymasks, 0):
        for z in (*zmasks, 0):
            push(z + y + 1, 1, z + y)
    yield None
    for z in (*zmasks, 0):
        for y in ymasks:
            own[z + y, :, cols] = fold(z + y, [z + y]).astype(BF16)
            push(z + y, y, z + y + 1)
    yield None
    for z in zmasks:
        own[z, :, cols] = fold(z, [z, *(z + y + 1 for y in ymasks)]).astype(BF16)
        push(z, z, z + 1)
    yield None
    yield fold(0, [0, *(y + 1 for y in ymasks), *(z + 1 for z in zmasks)])


def mix_kernel(
    ranks_ep,
    ranks_tp,
    partial_ref,
    tokens_ref,
    gain_ref,
    vector_ref,
    routes_ref,
    portions_ref,
    sgate_ref,
    sup_ref,
    sdown_hbm,
    gate_hbm,
    up_hbm,
    down_hbm,
    out_ref,
    attn_in,
    residual_ref,
    gathered,
    hidden_ref,
    terms,
    terms_in,
    shared,
    shared_in,
    last,
    last_in,
    gate_w,
    up_w,
    down_w,
    sdown_w,
    load_sem,
    tp_send,
    tp_recv,
    ag_send,
    ag_recv,
    rs_send,
    rs_recv,
    sh_send,
    sh_recv,
    out_send,
    out_recv,
):
    me = lax.axis_index("ep")
    my_tp = lax.axis_index("tp")
    row_count, width = tokens_ref.shape
    experts = gate_w.shape[0]
    table_width = gathered.shape[2] - width
    all_rows = ranks_ep * row_count
    chips = ranks_ep // 2
    across = 1 << (chips.bit_length() - 1) // 2
    zmasks = [m * 2 * across for m in range(chips // across - 1, 0, -1)]
    ymasks = [m * 2 for m in range(across - 1, 0, -1)]

    def flip(mask):
        index = me
        weight = 1
        while weight <= mask:
            if mask & weight:
                index = index + (1 - 2 * ((me // weight) % 2)) * weight
            weight = weight * 2
        return index

    loads = []
    for i, (source, target) in enumerate(
        ((gate_hbm, gate_w), (up_hbm, up_w), (down_hbm, down_w), (sdown_hbm, sdown_w))
    ):
        load = pltpu.make_async_copy(source, target, load_sem.at[i])
        load.start()
        loads.append(load)

    barrier = pltpu.get_barrier_semaphore()
    for mask in (*zmasks, *ymasks, 1):
        pl.semaphore_signal(barrier, inc=1, device_id={"ep": flip(mask)}, device_id_type=MESH)
    for step in range(1, ranks_tp):
        pl.semaphore_signal(
            barrier, inc=1, device_id={"tp": lax.rem(my_tp + step, ranks_tp)}, device_id_type=MESH
        )
    pl.semaphore_wait(barrier, len(zmasks) + len(ymasks) + ranks_tp)

    swaps = []
    for step in range(1, ranks_tp):
        swap = pltpu.make_async_remote_copy(
            src_ref=partial_ref,
            dst_ref=attn_in.at[step - 1],
            send_sem=tp_send.at[step - 1],
            recv_sem=tp_recv.at[step - 1],
            device_id={"tp": lax.rem(my_tp + step, ranks_tp)},
            device_id_type=MESH,
        )
        swap.start()
        swaps.append(swap)

    lane = lax.broadcasted_iota(jnp.int32, (row_count, table_width), 1)
    stride = table_width // 2
    table = jnp.zeros((row_count, table_width), F32)
    for k in range(routes_ref.shape[1]):
        named = routes_ref[:, k : k + 1]
        portion = portions_ref[:, k : k + 1]
        high = portion.astype(BF16).astype(F32)
        table = jnp.where(lane == named, high, table)
        table = jnp.where(lane == named + stride, portion - high, table)
    gathered[0, :, width:] = table.astype(BF16)

    residual = partial_ref[...].astype(F32)
    for step in range(1, ranks_tp):
        swaps[step - 1].wait()
        residual = residual + attn_in[step - 1].astype(F32)
    residual = residual + tokens_ref[...].astype(F32)
    residual_ref[...] = residual
    normed = (
        residual
        * lax.rsqrt(jnp.mean(residual * residual, axis=-1, keepdims=True) + epsilon)
        * gain_ref[...]
    ).astype(BF16)
    gathered[0, :, :width] = normed

    sent = []
    arrivals = {}

    def share(block, goal):
        slot = block ^ goal
        copy = pltpu.make_async_remote_copy(
            src_ref=gathered.at[block],
            dst_ref=gathered.at[slot],
            send_sem=ag_send.at[len(sent)],
            recv_sem=ag_recv.at[slot],
            device_id={"ep": flip(goal)},
            device_id_type=MESH,
        )
        copy.start()
        sent.append(copy)
        arrivals[slot] = copy

    for mask in (*zmasks, *ymasks, 1):
        share(0, mask)
    mix_gate = jax.nn.sigmoid(
        jnp.sum(normed.astype(F32) * vector_ref[...].astype(F32), axis=1, keepdims=True)
    )
    for y in ymasks:
        arrivals[y].wait_recv()
        share(y, 1)
    for z in zmasks:
        arrivals[z].wait_recv()
        for y in ymasks:
            share(z, y)
        share(z, 1)
    for z in zmasks:
        for y in ymasks:
            arrivals[z + y].wait_recv()
            share(z + y, 1)
    for z in (*zmasks, 0):
        for y in (*ymasks, 0):
            arrivals[z + y + 1].wait_recv()

    shared_cols = sgate_ref.shape[1]
    depth = sgate_ref.shape[0]
    feature_at = pl.ds(pl.multiple_of(me * (width // ranks_ep) // depth * depth, depth), depth)
    features = gathered[:, :, feature_at].reshape(all_rows, depth)
    for i, part in enumerate((sgate_ref, sup_ref)):
        shared[:, :, i * shared_cols : (i + 1) * shared_cols] = (
            jnp.dot(features, part[...], preferred_element_type=F32)
            .astype(BF16)
            .reshape(ranks_ep, row_count, shared_cols)
        )
    shared_sent = []
    shared_rounds = reduce_rounds(
        shared,
        shared_in,
        flip,
        zmasks,
        ymasks,
        slice(None),
        sh_send,
        sh_recv,
        shared_sent,
    )
    next(shared_rounds)
    rows = gathered[:, :, :width].reshape(all_rows, width)
    route_cols = gathered[:, :, width:].reshape(all_rows, table_width).astype(F32)
    lanes = lax.broadcasted_iota(jnp.int32, route_cols.shape, 1)
    loads[0].wait()
    loads[1].wait()
    scales = []
    for j in range(experts):
        wanted = me * experts + j
        chosen = jnp.where((lanes == wanted) | (lanes == wanted + stride), route_cols, 0.0)
        scales.append(jnp.sum(chosen, axis=1, keepdims=True))
        gate_val = jnp.dot(rows, gate_w[j], preferred_element_type=F32)
        up_val = jnp.dot(rows, up_w[j], preferred_element_type=F32)
        hidden_ref[j] = (gate_val * jax.nn.sigmoid(gate_val) * up_val).astype(BF16)
    next(shared_rounds)
    loads[2].wait()
    loads[3].wait()
    half = width // 2
    term_sent = []
    rounds = []
    for s in range(2):
        cols = slice(s * half, (s + 1) * half)
        term = jnp.zeros((all_rows, half), F32)
        for j in range(experts):
            term = term + scales[j] * jnp.dot(
                hidden_ref[j], down_w[j, :, cols], preferred_element_type=F32
            )
        terms[:, :, cols] = term.astype(BF16).reshape(ranks_ep, row_count, half)
        term_sent.append([])
        rounds.append(
            reduce_rounds(
                terms,
                terms_in,
                flip,
                zmasks,
                ymasks,
                cols,
                rs_send.at[s],
                rs_recv.at[s],
                term_sent[s],
            )
        )
        next(rounds[s])
        if s == 0:
            next(shared_rounds)
    for turn in range(2):
        for s in range(2):
            next(rounds[s])
    total = next(shared_rounds)
    gate_sum = total[:, :shared_cols]
    up_sum = total[:, shared_cols:]
    shared_hidden = (gate_sum * jax.nn.sigmoid(gate_sum) * up_sum).astype(BF16)
    shared_term = mix_gate * jnp.dot(shared_hidden, sdown_w[...], preferred_element_type=F32)
    for s in range(2):
        cols = slice(s * half, (s + 1) * half)
        last[:, cols] = (next(rounds[s]) + shared_term[:, cols]).astype(BF16)
    quarter = width // ranks_tp

    def quarter_of(index):
        return pl.ds(pl.multiple_of(index * quarter, quarter), quarter)

    ends = []
    for step in range(1, ranks_tp):
        goal = lax.rem(my_tp + step, ranks_tp)
        end = pltpu.make_async_remote_copy(
            src_ref=last.at[:, quarter_of(goal)],
            dst_ref=last_in.at[step - 1],
            send_sem=out_send.at[step - 1],
            recv_sem=out_recv.at[step - 1],
            device_id={"tp": goal},
            device_id_type=MESH,
        )
        end.start()
        ends.append(end)
    for copy in (*sent, *shared_sent, *term_sent[0], *term_sent[1]):
        copy.wait_send()
    result = residual_ref[:, quarter_of(my_tp)] + last[:, quarter_of(my_tp)].astype(F32)
    for step in range(1, ranks_tp):
        ends[step - 1].wait()
        result = result + last_in[step - 1].astype(F32)
    out_ref[...] = result.astype(BF16)


def mix(
    ranks_ep,
    ranks_tp,
    attn_term,
    tokens,
    ffn_gain,
    gate_vector,
    routes,
    route_weights,
    shared_gate,
    shared_up,
    shared_down,
    expert_gate,
    expert_up,
    expert_down,
):
    row_count, width = tokens.shape
    grid = (ranks_ep, row_count)
    experts, _, hidden = expert_gate.shape
    shared_cols = shared_gate.shape[1]
    quarter = width // ranks_tp
    table_width = -(-2 * ranks_ep * experts // LANES) * LANES
    swaps = max(ranks_tp - 1, 1)
    vmem = pl.BlockSpec(memory_space=pltpu.VMEM)
    anywhere = pl.BlockSpec(memory_space=pl.ANY)
    dma = pltpu.SemaphoreType.DMA
    return pl.pallas_call(
        functools.partial(mix_kernel, ranks_ep, ranks_tp),
        out_shape=jax.ShapeDtypeStruct((row_count, quarter), BF16),
        in_specs=[vmem] * 8 + [anywhere] * 4,
        out_specs=vmem,
        scratch_shapes=[
            pltpu.VMEM((swaps, row_count, width), BF16),
            pltpu.VMEM((row_count, width), F32),
            pltpu.VMEM((*grid, width + table_width), BF16),
            pltpu.VMEM((experts, ranks_ep * row_count, hidden), BF16),
            pltpu.VMEM((*grid, width), BF16),
            pltpu.VMEM((*grid, width), BF16),
            pltpu.VMEM((*grid, 2 * shared_cols), BF16),
            pltpu.VMEM((*grid, 2 * shared_cols), BF16),
            pltpu.VMEM((row_count, width), BF16),
            pltpu.VMEM((swaps, row_count, quarter), BF16),
            pltpu.VMEM(expert_gate.shape, BF16),
            pltpu.VMEM(expert_up.shape, BF16),
            pltpu.VMEM(expert_down.shape, BF16),
            pltpu.VMEM(shared_down.shape, BF16),
            dma((4,)),
            dma((swaps,)),
            dma((swaps,)),
            dma((ranks_ep,)),
            dma((ranks_ep,)),
            dma((2, ranks_ep)),
            dma((2, ranks_ep)),
            dma((ranks_ep,)),
            dma((ranks_ep,)),
            dma((swaps,)),
            dma((swaps,)),
        ],
        compiler_params=pltpu.CompilerParams(
            collective_id=0, has_side_effects=True, vmem_limit_bytes=60 * 2**20
        ),
    )(
        attn_term,
        tokens,
        ffn_gain.reshape(1, width),
        gate_vector.reshape(1, width),
        routes,
        route_weights,
        shared_gate,
        shared_up,
        shared_down,
        expert_gate,
        expert_up,
        expert_down,
    )


def shards(
    ranks_ep,
    ranks_tp,
    tokens,
    lengths,
    cache,
    attn_gain,
    query_weight,
    key_weight,
    value_weight,
    stick_bias,
    out_weight,
    ffn_gain,
    routes,
    route_weights,
    expert_gate,
    expert_up,
    expert_down,
    shared_gate,
    shared_up,
    shared_down,
    gate_vector,
):
    row_count = tokens.shape[0]
    normed = rms_scale(tokens, attn_gain).astype(BF16)
    queries = jnp.dot(normed, query_weight, preferred_element_type=F32).astype(BF16)
    key_rows = jnp.dot(normed, key_weight, preferred_element_type=F32).astype(BF16)
    value_rows = jnp.dot(normed, value_weight, preferred_element_type=F32).astype(BF16)
    heads = key_weight.shape[1] // HEAD_DIM
    new_kv = jnp.stack(
        [
            key_rows.reshape(row_count, heads, HEAD_DIM),
            value_rows.reshape(row_count, heads, HEAD_DIM),
        ],
        axis=2,
    ).reshape(row_count, heads * 2 * HEAD_DIM)
    group = queries.shape[1] // HEAD_DIM // heads
    same = jnp.eye(heads, dtype=jnp.bool_)
    spread = jnp.where(
        same[None, :, None, :, None],
        queries.reshape(row_count, heads, group, 1, HEAD_DIM),
        jnp.zeros((), BF16),
    )
    spread = jnp.pad(spread, ((0, 0),) * 4 + ((0, HEAD_DIM),))
    query_grid = spread.reshape(row_count, heads * group, heads * 2 * HEAD_DIM)
    mixed = attend(query_grid, lengths, stick_bias, cache)
    mixed = mixed.reshape(row_count, heads, group, heads, 2 * HEAD_DIM)[..., HEAD_DIM:]
    heads_out = jnp.sum(jnp.where(same[None, :, None, :, None], mixed, 0.0), axis=3).astype(BF16)
    attn_term = jnp.dot(
        heads_out.reshape(row_count, -1), out_weight, preferred_element_type=F32
    ).astype(BF16)
    depth = shared_gate.shape[0]
    if depth % LANES:
        slot = lax.axis_index("ep") * depth % LANES
        wide = jnp.zeros((LANES, shared_gate.shape[1]), BF16)
        shared_gate = lax.dynamic_update_slice_in_dim(wide, shared_gate, slot, 0)
        shared_up = lax.dynamic_update_slice_in_dim(wide, shared_up, slot, 0)
    layer_out = mix(
        ranks_ep,
        ranks_tp,
        attn_term,
        tokens,
        ffn_gain,
        gate_vector,
        routes,
        route_weights,
        shared_gate,
        shared_up,
        shared_down,
        expert_gate,
        expert_up,
        expert_down,
    )
    return (layer_out, new_kv)


def solution(mesh):
    placed = (
        P("ep", None),
        P("ep"),
        P("ep", None, "tp"),
        P(),
        P(None, "tp"),
        P(None, "tp"),
        P(None, "tp"),
        P("tp"),
        P("tp", None),
        P(),
        P("ep", None),
        P("ep", None),
        P("ep", None, "tp"),
        P("ep", None, "tp"),
        P("ep", "tp", None),
        P("ep", "tp"),
        P("ep", "tp"),
        P("tp", None),
        P(),
    )
    return jax.shard_map(
        functools.partial(shards, mesh.shape["ep"], mesh.shape["tp"]),
        mesh=mesh,
        in_specs=placed,
        out_specs=(P("ep", "tp"), P("ep", "tp")),
        check_vma=False,
    )
```

time: 69.7 us -> 63.4 us (0.910)
  Pallas kernels: 56.4 us -> 51 us
  other arithmetic: 2.33 us -> 1.57 us
    pallas_call x1, Pallas kernels: 47.1 us -> 41.7 us  [mix(): pl.pallas_call(functools.partial(mix_kernel, ranks_ep, ranks_tp), out_sha...]
    another operation x3 -> x0, local copies, waits for them, and re-layouts: 1.42 us -> none  [the longest x2 0.72 us: attend(): bias_rows = jnp.tile(bias, seqs).reshape(seqs * heads, 1)]
    unnamed x21 -> x19, local copies, waits for them, and re-layouts: 1.43 us -> 2.77 us
where the time goes in v2:
time: 63.4 us; the launch traced here: 63 us
  Pallas kernels  51 us (80%)
  local copies, waits for them, and re-layouts  6.17 us (10%)
  matrix products  3.56 us (6%)
  other arithmetic  1.57 us (2%)
  between operations  0.77 us (1%)
    pallas_call x1, Pallas kernels, mix(): pl.pallas_call(functools.partial(mix_kernel, ranks_ep, ranks_tp), out_sha...  41.7 us
    pallas_call x1, Pallas kernels, attend(): pl.pallas_call(functools.partial(attend_kernel, 2), out_shape=jax.ShapeDt...  9.26 us
    unnamed x19, local copies, waits for them, and re-layouts  2.77 us
    dot_general x1, matrix products, shards(): jnp.dot(normed, query_weight, preferred_element_type=F32).astype(BF16)  2.07 us

profile of v2, /device:TPU:0, one launch (start us, length us, event | category | flops | bytes accessed | tf_op | source)
XLA Modules:
  0.0 63.0 jit_solution(17116946266721015720)
XLA Ops:
  0.6 0.0 copy-start
  0.6 1.1 %fusion = f32[16]{0:T(128)S(1)} fusion(bf16[16,2048]{1,0:T(8,128)(2,1)} %tokens_ref.1), kind=kLoop, calls=%fused_computation.6 | loop fusion | flops 98288 | bytes 65600 | tf_op jit(solution)/shard_map/reduce_sum | solution.py:22
  1.8 2.1 %convolution_convert_fusion.1 = bf16[16,512]{1,0:T(8,128)(2,1)S(1)} fusion(bf16[2048,512]{1,0:T(8,128)(2,1)} %param.23, bf16[16,2048]{1,0:T(8,128)(2,1)} %tokens_ref.1, f32[2048]{0:T(1024)} %param.22, f32[16]{0:T(128)S(1)} %add_rsqrt_fusion), kind=kOutput, calls=%fused_computation.1 | convolution fusion | flops 33693696 | bytes 2187328 | tf_op jit(solution)/shard_map/dot_general | solution.py:495
  3.8 0.1 broadcast_in_dim.39
  4.0 0.1 broadcast_select_fusion
  4.1 0.1 pad.4
  4.2 0.7 %reshape.40.query_ref = bf16[16,8,256]{2,1,0:T(8,128)(2,1)} reshape(bf16[16,2,4,2,128]{4,3,2,1,0:T(2,128)(2,1)S(1)} %pad.4) | data formatting | bytes 131072 | tf_op jit(solution)/shard_map/reshape | solution.py:514
  4.8 9.3 %shard_map.194 = f32[16,8,256]{2,1,0:T(8,128)} custom-call(bf16[16,8,256]{2,1,0:T(8,128)(2,1)} %reshape.40.query_ref, s32[16]{0:T(128)} %span_ref.1, f32[8]{0:T(128)} %bias_ref.1, bf16[16,1024,256]{2,1,0:T(8,128)(2,1)} %cache_ref.1), custom_call_target="tpu_custom_call" | custom-call | tf_op jit(solution)/shard_map/pallas_call | solution.py:82
  14.1 0.0 copy-start.5
  14.1 0.0 copy-start.6
  14.1 0.0 copy-start.7
  14.1 1.0 %reshape.41 = f32[16,2,4,2,128]{4,3,2,1,0:T(2,128)S(1)} reshape(f32[16,8,256]{2,1,0:T(8,128)} %shard_map.194) | data formatting | bytes 262144 | tf_op jit(solution)/shard_map/reshape | solution.py:516
  15.1 0.3 fusion.3
  15.4 0.1 convert_element_type.31
  15.5 0.0 copy-done
  15.5 1.0 %convolution_convert_fusion.partial_ref = bf16[16,2048]{1,0:T(8,128)(2,1)} fusion(bf16[16,512]{1,0:T(8,128)(2,1)S(1)} %convert_element_type.31, bf16[512,2048]{1,0:T(8,128)(2,1)S(1)} %copy-done), kind=kOutput, calls=%fused_computation | convolution fusion | flops 33587200 | bytes 2179072 | tf_op jit(solution)/shard_map/dot_general | solution.py:518
  16.5 0.0 copy-done.5
  16.5 0.7 %copy.21.routes_ref = s32[16,6]{1,0:T(8,128)} copy(s32[16,6]{0,1:T(8,128)S(1)} %copy-done.5) | data formatting | bytes 768 | tf_op args[10]
  17.2 0.0 copy-done.6
  17.2 0.7 %copy.22.portions_ref = f32[16,6]{1,0:T(8,128)} copy(f32[16,6]{0,1:T(8,128)S(1)} %copy-done.6) | data formatting | bytes 768 | tf_op args[11]
  17.9 0.0 copy-done.7
  17.9 0.6 reshape.43.vector_ref
  18.5 41.7 %shard_map.195 = bf16[16,1024]{1,0:T(8,128)(2,1)} custom-call(bf16[16,2048]{1,0:T(8,128)(2,1)} %convolution_convert_fusion.partial_ref, bf16[16,2048]{1,0:T(8,128)(2,1)} %tokens_ref.1, f32[1,2048]{1,0:T(1,128)} %bitcast.6, bf16[1,2048]{1,0:T(2,128)(2,1)} %reshape.43.vector_ref, s32[16,6]{1,0:T(8,128)} %copy.21.routes_ref, f32[16,6]{1,0:T(8,128)} %copy.22.portions_ref, ...), custom_call_target="tpu_custom_call" | custom-call | tf_op jit(solution)/shard_map/pallas_call | solution.py:419
  60.2 0.0 copy-done.1
  60.2 0.0 copy-done.2
  60.3 0.0 copy-done.4
  60.3 0.2 convolution_convert_fusion.3
  60.5 0.1 stack_reshape.6
  60.6 0.2 convolution_convert_fusion.2
  60.8 0.1 stack_reshape.7
  61.0 0.7 %reshape.44 = bf16[16,256]{1,0:T(8,128)(2,1)} reshape(bf16[16,2,2,64]{3,2,1,0:T(2,128)(2,1)S(1)} %copy.23) | data formatting | bytes 16384 | tf_op jit(solution)/shard_map/reshape | solution.py:505
  61.7 1.4 %copy.25 = bf16[16,1024]{1,0:T(8,128)(2,1)} copy(bf16[16,1024]{1,0:T(8,128)(2,1)} %shard_map.195) | data formatting | bytes 65536
  (9 shorter events, 0.1 us)
Async XLA Ops:
  0.6 14.9 %copy-start = (bf16[512,2048]{1,0:T(8,128)(2,1)S(1)}, bf16[512,2048]{1,0:T(8,128)(2,1)}, u32[]{:S(2)}) copy-start(bf16[512,2048]{1,0:T(8,128)(2,1)} %param.27) | copy-start | bytes 6291460
  14.1 2.4 %copy-start.5 = (s32[16,6]{0,1:T(8,128)S(1)}, s32[16,6]{0,1:T(8,128)}, u32[]{:S(2)}) copy-start(s32[16,6]{0,1:T(8,128)} %param.29) | copy-start | bytes 1156
  14.1 3.1 %copy-start.6 = (f32[16,6]{0,1:T(8,128)S(1)}, f32[16,6]{0,1:T(8,128)}, u32[]{:S(2)}) copy-start(f32[16,6]{0,1:T(8,128)} %param.30) | copy-start | bytes 1156
  14.1 3.8 %copy-start.7 = (bf16[2048]{0:T(1024)(128)(2,1)S(1)}, bf16[2048]{0:T(1024)(128)(2,1)}, u32[]{:S(2)}) copy-start(bf16[2048]{0:T(1024)(128)(2,1)} %param.37) | copy-start | bytes 12292
  18.5 41.7 %copy-start.1 = (bf16[16,2048]{1,0:T(8,128)(2,1)S(1)}, bf16[16,2048]{1,0:T(8,128)(2,1)}, u32[]{:S(2)}) copy-start(bf16[16,2048]{1,0:T(8,128)(2,1)} %tokens_ref.1) | copy-start | bytes 196612
  18.5 41.8 %copy-start.2 = (bf16[2048,128]{1,0:T(8,128)(2,1)S(1)}, bf16[2048,128]{1,0:T(8,128)(2,1)}, u32[]{:S(2)}) copy-start(bf16[2048,128]{1,0:T(8,128)(2,1)} %param.24) | copy-start | bytes 1572868
  18.5 41.8 %copy-start.4 = (f32[2048]{0:T(1024)S(1)}, f32[2048]{0:T(1024)}, u32[]{:S(2)}) copy-start(f32[2048]{0:T(1024)} %param.22) | copy-start | bytes 24580
  18.5 42.1 %copy-start.3 = (bf16[2048,128]{1,0:T(8,128)(2,1)S(1)}, bf16[2048,128]{1,0:T(8,128)(2,1)}, u32[]{:S(2)}) copy-start(bf16[2048,128]{1,0:T(8,128)(2,1)} %param.25) | copy-start | bytes 1572868

commit v3 on v2

--- a/solution.py
+++ b/solution.py
@@ -24,8 +24,11 @@
     )
 
 
-def attend_kernel(groups, query_ref, span_ref, bias_ref, cache_ref, out_ref, held, logits, sems):
-    seqs, heads, _ = query_ref.shape
+def attend_kernel(groups, query_ref, span_ref, bias_ref, cache_ref, out_ref, held, logits, spread, sems):
+    seqs, heads, _ = spread.shape
+    tiles = spread.shape[2] // LANES
+    group = heads // tiles
+    first_half = lax.broadcasted_iota(jnp.int32, (seqs, LANES), 1) < HEAD_DIM
     length = cache_ref.shape[1]
     width = 256
     count = length // width
@@ -34,6 +37,13 @@
         copy = pltpu.make_async_copy(cache_ref.at[s], held.at[s], sems.at[s])
         copy.start()
         copies.append(copy)
+    spread[...] = jnp.zeros_like(spread)
+    for h in range(heads):
+        pair = query_ref[:, h // 2 * LANES : (h // 2 + 1) * LANES].astype(F32)
+        if h % 2:
+            pair = pltpu.roll(pair, HEAD_DIM, 1)
+        tile = h // group * LANES
+        spread[:, h, tile : tile + LANES] = jnp.where(first_half, pair, 0.0)
     table = (
         lax.broadcasted_iota(jnp.int32, (width, width), 0)
         >= lax.broadcasted_iota(jnp.int32, (width, width), 1)
@@ -45,7 +55,7 @@
         for s in range(first, first + per_group):
             copies[s].wait()
             logits[s * heads : (s + 1) * heads, :] = lax.dot_general(
-                query_ref[s], held[s], (((1,), (1,)), ((), ())), preferred_element_type=F32
+                spread[s].astype(BF16), held[s], (((1,), (1,)), ((), ())), preferred_element_type=F32
             )
         span = slice(first * heads, first * heads + rows)
         row = lax.broadcasted_iota(jnp.int32, (rows, 1), 0)
@@ -67,30 +77,39 @@
             carried = carried + jnp.sum(soft, axis=1, keepdims=True)
             logits[span, cols] = weight
         for s in range(first, first + per_group):
-            out_ref[s] = jnp.dot(
+            spread[s] = jnp.dot(
                 logits[s * heads : (s + 1) * heads, :].astype(BF16),
                 held[s],
                 preferred_element_type=F32,
             )
-
-
-def attend(query_grid, lengths, bias, cache):
-    seqs, heads, lanes = query_grid.shape
-    length = cache.shape[1]
+    for i in range(heads // 2):
+        pair = []
+        for h in (2 * i, 2 * i + 1):
+            tile = h // group * LANES
+            pair.append(spread[:, h, tile : tile + LANES])
+        both = jnp.where(first_half, pltpu.roll(pair[0], HEAD_DIM, 1), pair[1])
+        out_ref[:, i * LANES : (i + 1) * LANES] = both.astype(BF16)
+
+
+def attend(queries, lengths, bias, cache):
+    seqs = queries.shape[0]
+    heads = queries.shape[1] // HEAD_DIM
+    length, lanes = cache.shape[1:]
     smem = pl.BlockSpec(memory_space=pltpu.SMEM)
     vmem = pl.BlockSpec(memory_space=pltpu.VMEM)
     return pl.pallas_call(
         functools.partial(attend_kernel, 2),
-        out_shape=jax.ShapeDtypeStruct((seqs, heads, lanes), F32),
+        out_shape=jax.ShapeDtypeStruct(queries.shape, BF16),
         in_specs=[vmem, smem, smem, pl.BlockSpec(memory_space=pl.ANY)],
         out_specs=vmem,
         scratch_shapes=[
             pltpu.VMEM((seqs, length, lanes), BF16),
             pltpu.VMEM((seqs * heads, length), F32),
+            pltpu.VMEM((seqs, heads, lanes), F32),
             pltpu.SemaphoreType.DMA((seqs,)),
         ],
         compiler_params=pltpu.CompilerParams(vmem_limit_bytes=60 * 2**20),
-    )(query_grid, lengths, bias, cache)
+    )(queries, lengths, bias, cache)
 
 
 def reduce_rounds(own, landing, flip, zmasks, ymasks, cols, send_sem, recv_sem, sent):
@@ -226,9 +245,11 @@
     lane = lax.broadcasted_iota(jnp.int32, (row_count, table_width), 1)
     stride = table_width // 2
     table = jnp.zeros((row_count, table_width), F32)
-    for k in range(routes_ref.shape[1]):
-        named = routes_ref[:, k : k + 1]
-        portion = portions_ref[:, k : k + 1]
+    route_ids = jnp.transpose(routes_ref[...])
+    portions = jnp.transpose(portions_ref[...])
+    for k in range(routes_ref.shape[0]):
+        named = route_ids[:, k : k + 1]
+        portion = portions[:, k : k + 1]
         high = portion.astype(BF16).astype(F32)
         table = jnp.where(lane == named, high, table)
         table = jnp.where(lane == named + stride, portion - high, table)
@@ -267,7 +288,7 @@
     for mask in (*zmasks, *ymasks, 1):
         share(0, mask)
     mix_gate = jax.nn.sigmoid(
-        jnp.sum(normed.astype(F32) * vector_ref[...].astype(F32), axis=1, keepdims=True)
+        jnp.sum(normed.astype(F32) * vector_ref[...].astype(F32).reshape(1, width), axis=1, keepdims=True)
     )
     for y in ymasks:
         arrivals[y].wait_recv()
@@ -387,7 +408,7 @@
     for step in range(1, ranks_tp):
         ends[step - 1].wait()
         result = result + last_in[step - 1].astype(F32)
-    out_ref[...] = result.astype(BF16)
+    out_ref[...] = result
 
 
 def mix(
@@ -418,7 +439,7 @@
     dma = pltpu.SemaphoreType.DMA
     return pl.pallas_call(
         functools.partial(mix_kernel, ranks_ep, ranks_tp),
-        out_shape=jax.ShapeDtypeStruct((row_count, quarter), BF16),
+        out_shape=jax.ShapeDtypeStruct((row_count, quarter), F32),
         in_specs=[vmem] * 8 + [anywhere] * 4,
         out_specs=vmem,
         scratch_shapes=[
@@ -455,9 +476,9 @@
         attn_term,
         tokens,
         ffn_gain.reshape(1, width),
-        gate_vector.reshape(1, width),
-        routes,
-        route_weights,
+        gate_vector,
+        routes.T,
+        route_weights.T,
         shared_gate,
         shared_up,
         shared_down,
@@ -503,20 +524,9 @@
         ],
         axis=2,
     ).reshape(row_count, heads * 2 * HEAD_DIM)
-    group = queries.shape[1] // HEAD_DIM // heads
-    same = jnp.eye(heads, dtype=jnp.bool_)
-    spread = jnp.where(
-        same[None, :, None, :, None],
-        queries.reshape(row_count, heads, group, 1, HEAD_DIM),
-        jnp.zeros((), BF16),
-    )
-    spread = jnp.pad(spread, ((0, 0),) * 4 + ((0, HEAD_DIM),))
-    query_grid = spread.reshape(row_count, heads * group, heads * 2 * HEAD_DIM)
-    mixed = attend(query_grid, lengths, stick_bias, cache)
-    mixed = mixed.reshape(row_count, heads, group, heads, 2 * HEAD_DIM)[..., HEAD_DIM:]
-    heads_out = jnp.sum(jnp.where(same[None, :, None, :, None], mixed, 0.0), axis=3).astype(BF16)
+    heads_out = attend(queries, lengths, stick_bias, cache)
     attn_term = jnp.dot(
-        heads_out.reshape(row_count, -1), out_weight, preferred_element_type=F32
+        heads_out, out_weight, preferred_element_type=F32
     ).astype(BF16)
     depth = shared_gate.shape[0]
     if depth % LANES:
@@ -540,7 +550,7 @@
         expert_up,
         expert_down,
     )
-    return (layer_out, new_kv)
+    return (layer_out.astype(BF16), new_kv)
 
 
 def solution(mesh):

time: 63.4 us -> 60.4 us (0.953)
  local copies, waits for them, and re-layouts: 6.17 us -> 0.89 us
  matrix products: 3.56 us -> 4.89 us
  other arithmetic: 1.57 us -> 2.63 us
    unnamed x19 -> x10, local copies, waits for them, and re-layouts: 2.77 us -> 0.02 us
    reshape x3 -> x0, local copies, waits for them, and re-layouts: 2.26 us -> none  [the longest x1 0.98 us: shards(): mixed.reshape(row_count, heads, group, heads, 2 * HEAD_DIM)[..., HEAD_DIM:]]
    convert_element_type x0 -> x1, other arithmetic: none -> 1.46 us  [shards(): return (layer_out.astype(BF16), new_kv)]
    dot_general x1, matrix products: 1 us -> 1.72 us  [shards(): jnp.dot(heads_out, out_weight, preferred_element_type=F32).astype(BF16)]
where the time goes in v3:
time: 60.4 us; the launch traced here: 60.1 us
  Pallas kernels  51 us (84%)
  matrix products  4.89 us (8%)
  other arithmetic  2.63 us (4%)
  local copies, waits for them, and re-layouts  0.89 us (1%)
  between operations  0.69 us (1%)
    pallas_call x1, Pallas kernels, mix(): pl.pallas_call(functools.partial(mix_kernel, ranks_ep, ranks_tp), out_sha...  41.7 us
    pallas_call x1, Pallas kernels, attend(): pl.pallas_call(functools.partial(attend_kernel, 2), out_shape=jax.ShapeDt...  9.26 us
    dot_general x1, matrix products, shards(): jnp.dot(normed, query_weight, preferred_element_type=F32).astype(BF16)  2.69 us
    dot_general x1, matrix products, shards(): jnp.dot(heads_out, out_weight, preferred_element_type=F32).astype(BF16)  1.72 us
    convert_element_type x1, other arithmetic, shards(): return (layer_out.astype(BF16), new_kv)  1.46 us

profile of v3, /device:TPU:0, one launch (start us, length us, event | category | flops | bytes accessed | tf_op | source)
XLA Modules:
  0.0 60.1 jit_solution(2759165085763370257)
XLA Ops:
  0.6 0.0 copy-start
  0.6 1.1 %fusion = f32[16]{0:T(128)S(1)} fusion(bf16[16,2048]{1,0:T(8,128)(2,1)} %tokens_ref.1), kind=kLoop, calls=%fused_computation.6 | loop fusion | flops 98288 | bytes 65600 | tf_op jit(solution)/shard_map/reduce_sum | solution.py:22
  1.8 2.7 %convolution_convert_fusion.1.query_ref = bf16[16,512]{1,0:T(8,128)(2,1)} fusion(bf16[2048,512]{1,0:T(8,128)(2,1)} %param.23, bf16[16,2048]{1,0:T(8,128)(2,1)} %tokens_ref.1, f32[2048]{0:T(1024)} %param.22, f32[16]{0:T(128)S(1)} %add_rsqrt_fusion), kind=kOutput, calls=%fused_computation.1 | convolution fusion | flops 33693696 | bytes 2187328 | tf_op jit(solution)/shard_map/dot_general | solution.py:516
  4.5 9.3 %shard_map.194 = bf16[16,512]{1,0:T(8,128)(2,1)} custom-call(bf16[16,512]{1,0:T(8,128)(2,1)} %convolution_convert_fusion.1.query_ref, s32[16]{0:T(128)} %span_ref.1, f32[8]{0:T(128)} %bias_ref.1, bf16[16,1024,256]{2,1,0:T(8,128)(2,1)} %cache_ref.1), custom_call_target="tpu_custom_call" | custom-call | tf_op jit(solution)/shard_map/pallas_call | solution.py:100
  13.7 0.0 copy-done
  13.7 1.7 %convolution_convert_fusion.partial_ref = bf16[16,2048]{1,0:T(8,128)(2,1)} fusion(bf16[16,512]{1,0:T(8,128)(2,1)} %shard_map.194, bf16[512,2048]{1,0:T(8,128)(2,1)S(1)} %copy-done), kind=kOutput, calls=%fused_computation | convolution fusion | flops 33587200 | bytes 2179072 | tf_op jit(solution)/shard_map/dot_general | solution.py:528
  15.5 0.0 copy-start.1
  15.5 0.0 copy-start.2
  15.5 0.0 copy-start.4
  15.5 0.0 copy-start.3
  15.5 41.7 %shard_map.195 = f32[16,1024]{1,0:T(8,128)} custom-call(bf16[16,2048]{1,0:T(8,128)(2,1)} %convolution_convert_fusion.partial_ref, bf16[16,2048]{1,0:T(8,128)(2,1)} %tokens_ref.1, f32[1,2048]{1,0:T(1,128)} %bitcast.8, bf16[2048]{0:T(1024)(128)(2,1)} %vector_ref.1, s32[6,16]{1,0:T(8,128)} %bitcast.9, f32[6,16]{1,0:T(8,128)} %bitcast.10, ...), custom_call_target="tpu_custom_call" | custom-call | tf_op jit(solution)/shard_map/pallas_call | solution.py:440
  57.2 1.5 %convert_element_type.25 = bf16[16,1024]{1,0:T(8,128)(2,1)} convert(f32[16,1024]{1,0:T(8,128)} %shard_map.195) | non-fusion elementwise | flops 16384 | bytes 98304 | tf_op jit(solution)/shard_map/convert_element_type | solution.py:553
  58.7 0.0 copy-done.1
  58.7 0.0 copy-done.2
  58.7 0.0 copy-done.4
  58.7 0.2 convolution_convert_fusion.2
  58.9 0.1 stack_reshape.7
  59.0 0.0 copy-done.3
  59.0 0.2 convolution_convert_fusion.3
  59.3 0.1 stack_reshape.6
  59.4 0.7 %reshape.20 = bf16[16,256]{1,0:T(8,128)(2,1)} reshape(bf16[16,2,2,64]{3,2,1,0:T(2,128)(2,1)S(1)} %copy.21) | data formatting | bytes 16384 | tf_op jit(solution)/shard_map/reshape | solution.py:526
  (3 shorter events, 0.1 us)
Async XLA Ops:
  0.6 13.1 %copy-start = (bf16[512,2048]{1,0:T(8,128)(2,1)S(1)}, bf16[512,2048]{1,0:T(8,128)(2,1)}, u32[]{:S(2)}) copy-start(bf16[512,2048]{1,0:T(8,128)(2,1)} %param.27) | copy-start | bytes 6291460
  15.5 43.2 %copy-start.1 = (bf16[16,2048]{1,0:T(8,128)(2,1)S(1)}, bf16[16,2048]{1,0:T(8,128)(2,1)}, u32[]{:S(2)}) copy-start(bf16[16,2048]{1,0:T(8,128)(2,1)} %tokens_ref.1) | copy-start | bytes 196612
  15.5 43.2 %copy-start.2 = (bf16[2048,128]{1,0:T(8,128)(2,1)S(1)}, bf16[2048,128]{1,0:T(8,128)(2,1)}, u32[]{:S(2)}) copy-start(bf16[2048,128]{1,0:T(8,128)(2,1)} %param.25) | copy-start | bytes 1572868
  15.5 43.2 %copy-start.4 = (f32[2048]{0:T(1024)S(1)}, f32[2048]{0:T(1024)}, u32[]{:S(2)}) copy-start(f32[2048]{0:T(1024)} %param.22) | copy-start | bytes 24580
  15.5 43.5 %copy-start.3 = (bf16[2048,128]{1,0:T(8,128)(2,1)S(1)}, bf16[2048,128]{1,0:T(8,128)(2,1)}, u32[]{:S(2)}) copy-start(bf16[2048,128]{1,0:T(8,128)(2,1)} %param.24) | copy-start | bytes 1572868
